TPU v7x, 32 devices: a whole 2x2x4 slice. The times are simulated.
32 devices in a mesh: sp: 8 (over z, x), tp: 4 (over y, core).
Axes of the slice: x: 2, y: 2, z: 4, core: 2. Of those that a mesh axis runs over, the one named last changes fastest.
Arguments:
- cotangent: bfloat16 [1024, 2048], P('sp'), may hold values from -6 to 6
- mixer_out: bfloat16 [1024, 2048], P('sp'), may hold values from -6 to 6
- expert_ids: int32 [1024, 2], P('sp'), may hold values from 0 to 7, all different within a row; in each aligned block of 128 rows (0 to 127, 128 to 255, ...) at most 64 rows name the same one
- route_weight: float32 [1024, 2], P('sp'), may hold values from 0.3 to 1.5
- saved_normalized: bfloat16 [1024, 2048], P('sp', 'tp'), may hold values from -6 to 6
- inverse_deviation: float32 [1024], P('sp'), may hold values from 0.3 to 3
- channel_norm_gain: float32 [2048], P('tp'), may hold values from 0.1 to 1.9
- taps: float32 [31, 2048], P(None, 'tp'), may hold values from -1 to 1
- proj_weight: bfloat16 [2048, 2048], P('tp'), may hold values from -0.125 to 0.125
- gate_weight: bfloat16 [8, 2048, 2048], P('sp', None, 'tp'), may hold values from -0.125 to 0.125
- up_weight: bfloat16 [8, 2048, 2048], P('sp', None, 'tp'), may hold values from -0.125 to 0.125
- down_weight: bfloat16 [8, 2048, 2048], P('sp', 'tp'), may hold values from -0.125 to 0.125
Outputs:
- grad_mixer_in: bfloat16 [1024, 2048], P('sp', 'tp')
- grad_proj: float32 [2048, 2048], P('sp', 'tp')
- grad_gate: bfloat16 [8, 2048, 2048], P('sp', None, 'tp')
- grad_up: bfloat16 [8, 2048, 2048], P('sp', None, 'tp')
- grad_down: bfloat16 [8, 2048, 2048], P('sp', 'tp')
Inputs may be any that keep to these rules, and one draw needn't show every extreme that they name: `expert_ids`: each row names 2 different experts. Within the rows of one index of sp no expert is named more than 64 times, a bound that some block reaches.
All inputs are finite; a program needn't handle non-finite values.
Results may differ from a plain program's by a relative error of at most 0.02.
Values may be sent and summed in bfloat16 or wider, within the bound.
A program may use at most 64 MiB of HBM per device.

v0:
```python
import functools

import jax
import jax.numpy as jnp
from jax import lax
from jax.experimental import pallas as pl
from jax.experimental.pallas import tpu as pltpu
from jax.sharding import PartitionSpec as P


def from_behind(value, axis, steps):
    count = lax.axis_size(axis)
    leading, last = (max(0, -steps), min(count, count - steps))
    return lax.ppermute(value, axis, [(source, source + steps) for source in range(leading, last)])


def route_table(expert_ids, route_weight, slot_start, slot_span, capacity, experts):
    onehot = (expert_ids[:, :, None] == jnp.arange(experts, dtype=jnp.int32)[None, None, :]).astype(
        jnp.int32
    )
    flat_hot = onehot.reshape(-1, experts)
    ranks = jnp.cumsum(flat_hot, axis=0) - flat_hot
    rank_pair = jnp.sum(ranks * flat_hot, axis=1).reshape(expert_ids.shape)
    slot_index = expert_ids * capacity + rank_pair
    targets = (
        jnp.arange(experts, dtype=jnp.int32)[:, None] * capacity
        + slot_start
        + jnp.arange(slot_span, dtype=jnp.int32)[None, :]
    ).reshape(-1)
    matched = slot_index[None, :, :] == targets[:, None, None]
    dispatch = jnp.any(matched, axis=2).astype(jnp.bfloat16)
    slot_weight = jnp.sum(jnp.where(matched, route_weight[None, :, :], 0.0), axis=(1, 2))
    return (dispatch, slot_weight)


def remote(source, target, send_sem, recv_sem, device):
    return pltpu.make_async_remote_copy(
        src_ref=source,
        dst_ref=target,
        send_sem=send_sem,
        recv_sem=recv_sem,
        device_id=device,
        device_id_type=pl.DeviceIdType.MESH,
    )


def dispatch_kernel(experts, groups, *refs):
    sent = refs[:2]
    held = refs[2:4]
    local_sem, far_send, far_recv, row_send, row_recv, pair_send, pair_recv = refs[4:]
    mine = lax.axis_index("sp")
    place = lax.axis_index("tp")
    chips = groups // 2
    chip, core = place // 2, place % 2
    sibling = chip * 2 + 1 - core

    def at_chip(step):
        return ((chip + step) % chips) * 2 + core

    barrier = pltpu.get_barrier_semaphore()

    def greet(step, carry):
        pl.semaphore_signal(barrier, inc=1, device_id=((mine + step) % experts, place),
                            device_id_type=pl.DeviceIdType.MESH)
        return carry

    lax.fori_loop(1, experts, greet, 0)
    for step in range(1, chips):
        pl.semaphore_signal(barrier, inc=1, device_id=(mine, at_chip(step)),
                            device_id_type=pl.DeviceIdType.MESH)
    pl.semaphore_signal(barrier, inc=1, device_id=(mine, sibling),
                        device_id_type=pl.DeviceIdType.MESH)
    pl.semaphore_wait(barrier, experts - 1 + chips)

    def far(a, step):
        peer = (mine + step) % experts
        return remote(sent[a].at[peer], held[a].at[mine, place],
                      far_send.at[a, step], far_recv.at[a, step], (peer, place))

    def row(a, step, hop):
        source = (mine + experts - step) % experts
        block = held[a].at[source, place]
        return remote(block, block, row_send.at[a, step, hop], row_recv.at[a, step, hop],
                      (mine, at_chip(hop)))

    def pair(a, step, hop):
        source = (mine + experts - step) % experts
        block = held[a].at[source, at_chip(chips - hop)]
        return remote(block, block, pair_send.at[a, step, hop], pair_recv.at[a, step, hop],
                      (mine, sibling))

    own = [
        pltpu.make_async_copy(sent[a].at[mine], held[a].at[mine, place], local_sem.at[a])
        for a in range(2)
    ]
    for a in range(2):
        own[a].start()
    for a in range(2):
        def start_far(step, carry, a=a):
            far(a, step).start()
            return carry

        lax.fori_loop(1, experts, start_far, 0)

    def pass_on(a, step):
        for hop in range(1, chips):
            row(a, step, hop).start()
        pair(a, step, 0).start()

    def pass_rows(a, step):
        for hop in range(1, chips):
            row(a, step, hop).wait_recv()
            pair(a, step, hop).start()

    for a in range(2):
        own[a].wait()
        pass_on(a, 0)
    for a in range(2):
        def arrive(step, carry, a=a):
            far(a, step).wait_recv()
            pass_on(a, step)
            pass_rows(a, step - 1)
            return carry

        lax.fori_loop(1, experts, arrive, 0)
        pass_rows(a, experts - 1)
    for a in range(2):
        def finish(step, carry, a=a):
            for hop in range(chips):
                pair(a, step, hop).wait()
                if hop:
                    row(a, step, hop).wait_send()
            return carry

        lax.fori_loop(0, experts, finish, 0)

        def finish_far(step, carry, a=a):
            far(a, step).wait_send()
            return carry

        lax.fori_loop(1, experts, finish_far, 0)


def dispatch_blocks(rows, grads, groups):
    experts, span, width = rows.shape
    chips = groups // 2
    full = jax.ShapeDtypeStruct((experts, groups, span, width), rows.dtype)
    dma = pltpu.SemaphoreType.DMA
    return pl.pallas_call(
        functools.partial(dispatch_kernel, experts, groups),
        out_shape=(full, full),
        in_specs=[pl.BlockSpec(memory_space=pltpu.VMEM)] * 2,
        out_specs=[pl.BlockSpec(memory_space=pltpu.VMEM)] * 2,
        scratch_shapes=[dma((2,))]
        + [dma((2, experts))] * 2
        + [dma((2, experts, chips))] * 4,
        compiler_params=pltpu.CompilerParams(
            collective_id=0, has_side_effects=True, vmem_limit_bytes=24 * 2**20
        ),
        cost_estimate=pl.CostEstimate(
            flops=0, bytes_accessed=40 * full.size, transcendentals=0
        ),
    )(rows, grads)


def home_kernel(experts, groups, partial, home, pair_in, row_out, row_in, total, *sems):
    pair_send, pair_recv, row_send, row_recv, far_send, far_recv = sems
    mine = lax.axis_index("sp")
    place = lax.axis_index("tp")
    chips = groups // 2
    chip, core = place // 2, place % 2
    sibling = chip * 2 + 1 - core

    def at_chip(step):
        return ((chip + step) % chips) * 2 + core

    barrier = pltpu.get_barrier_semaphore()

    def greet(step, carry):
        pl.semaphore_signal(barrier, inc=1, device_id=((mine + step) % experts, place),
                            device_id_type=pl.DeviceIdType.MESH)
        return carry

    lax.fori_loop(1, experts, greet, 0)
    for step in range(1, chips):
        pl.semaphore_signal(barrier, inc=1, device_id=(mine, at_chip(step)),
                            device_id_type=pl.DeviceIdType.MESH)
    pl.semaphore_signal(barrier, inc=1, device_id=(mine, sibling),
                        device_id_type=pl.DeviceIdType.MESH)
    pl.semaphore_wait(barrier, experts - 1 + chips)

    def pair(step, hop):
        owner = (mine + step + 1) % experts
        other = ((chip + hop) % chips) * 2 + 1 - core
        return remote(partial.at[other, owner], pair_in.at[hop, owner],
                      pair_send.at[step, hop], pair_recv.at[step, hop], (mine, sibling))

    def row(step, hop):
        owner = (mine + step + 1) % experts
        return remote(row_out.at[hop, owner], row_in.at[hop, owner],
                      row_send.at[step, hop], row_recv.at[step, hop], (mine, at_chip(hop)))

    def far(step):
        owner = (mine + step + 1) % experts
        return remote(total.at[owner], home.at[mine],
                      far_send.at[step], far_recv.at[step], (owner, place))

    def start_pair(step, carry):
        for hop in reversed(range(chips)):
            pair(step, hop).start()
        return carry

    lax.fori_loop(0, experts, start_pair, 0)

    def add_pair(step, hop):
        owner = (mine + step + 1) % experts
        pair(step, hop).wait_recv()
        return partial[at_chip(hop), owner].astype(jnp.float32) + pair_in[hop, owner].astype(
            jnp.float32
        )

    def send_rows(step):
        owner = (mine + step + 1) % experts
        for hop in range(1, chips):
            row_out[hop, owner] = add_pair(step, hop).astype(row_out.dtype)
            row(step, hop).start()

    def add_rows(step):
        owner = (mine + step + 1) % experts
        value = add_pair(step, 0)
        for hop in range(1, chips):
            row(step, hop).wait_recv()
            value = value + row_in[hop, owner].astype(jnp.float32)
        return value.astype(total.dtype)

    def advance(step, carry):
        send_rows(step)
        before = step - 1
        total[(mine + before + 1) % experts] = add_rows(before)
        far(before).start()
        return carry

    send_rows(0)
    lax.fori_loop(1, experts, advance, 0)
    home[mine] = add_rows(experts - 1)

    def finish(step, carry):
        for hop in range(chips):
            pair(step, hop).wait_send()
            if hop:
                row(step, hop).wait_send()
        return carry

    lax.fori_loop(0, experts, finish, 0)

    def finish_far(step, carry):
        far(step).wait()
        return carry

    lax.fori_loop(0, experts - 1, finish_far, 0)


def home_blocks(partial):
    groups, experts, capacity, share = partial.shape
    chips = groups // 2
    dma = pltpu.SemaphoreType.DMA
    blocks = pltpu.VMEM((chips, experts, capacity, share), partial.dtype)
    return pl.pallas_call(
        functools.partial(home_kernel, experts, groups),
        out_shape=jax.ShapeDtypeStruct((experts, capacity, share), partial.dtype),
        in_specs=[pl.BlockSpec(memory_space=pltpu.VMEM)],
        out_specs=pl.BlockSpec(memory_space=pltpu.VMEM),
        scratch_shapes=[blocks] * 3
        + [pltpu.VMEM((experts, capacity, share), partial.dtype)]
        + [dma((experts, chips))] * 4
        + [dma((experts,))] * 2,
        compiler_params=pltpu.CompilerParams(
            collective_id=1, has_side_effects=True, vmem_limit_bytes=24 * 2**20
        ),
        cost_estimate=pl.CostEstimate(
            flops=0, bytes_accessed=40 * partial.size, transcendentals=0
        ),
    )(partial)


def shards(
    cotangent,
    mixer_out,
    expert_ids,
    route_weight,
    saved_normalized,
    inverse_deviation,
    channel_norm_gain,
    taps,
    proj_weight,
    gate_weight,
    up_weight,
    down_weight,
):
    experts = lax.axis_size("sp")
    groups = lax.axis_size("tp")
    tok_rows, model_width = cotangent.shape
    capacity = groups * max(1, 4 * tok_rows // (experts * groups))
    slot_span = capacity // groups
    slot_start = lax.axis_index("tp") * slot_span
    dispatch, slot_weight = route_table(
        expert_ids, route_weight, slot_start, slot_span, capacity, experts
    )
    sent_rows = jnp.dot(dispatch, mixer_out, preferred_element_type=jnp.float32).astype(
        jnp.bfloat16
    )
    sent_grad = (
        slot_weight[:, None] * jnp.dot(dispatch, cotangent, preferred_element_type=jnp.float32)
    ).astype(jnp.bfloat16)
    sent_rows = sent_rows.reshape(experts, slot_span, model_width)
    sent_grad = sent_grad.reshape(experts, slot_span, model_width)
    normalized_input = saved_normalized.astype(jnp.float32)
    normalized_values = normalized_input * channel_norm_gain[None, :]
    gate_sig = jax.nn.sigmoid(normalized_values)
    act_conv = (normalized_values * gate_sig).astype(jnp.bfloat16)
    act_conv, sent_rows = lax.optimization_barrier((act_conv, sent_rows))
    every_act = lax.all_gather(act_conv, "sp", axis=0, tiled=True)
    routed_rows, routed_grad = dispatch_blocks(sent_rows, sent_grad, groups)
    full_table, unused_weight = route_table(
        expert_ids, route_weight, 0, capacity, capacity, experts
    )
    routed_rows = routed_rows.reshape(-1, model_width)
    routed_grad = routed_grad.reshape(-1, model_width)
    w_first = gate_weight[0]
    w_third = up_weight[0]
    w_second = down_weight[0]
    contract_last = (((1,), (1,)), ((), ()))
    contract_first = (((0,), (0,)), ((), ()))
    hidden_gate = jnp.dot(routed_rows, w_first, preferred_element_type=jnp.float32)
    hidden_up = jnp.dot(routed_rows, w_third, preferred_element_type=jnp.float32)
    sigma = jax.nn.sigmoid(hidden_gate)
    swish = hidden_gate * sigma
    activ = (swish * hidden_up).astype(jnp.bfloat16)
    grad_second = lax.dot_general(
        activ, routed_grad, contract_first, preferred_element_type=jnp.float32
    ).astype(jnp.bfloat16)
    grad_activ = lax.dot_general(
        routed_grad, w_second, contract_last, preferred_element_type=jnp.float32
    )
    grad_gpre = (grad_activ * hidden_up * sigma * (1.0 + hidden_gate * (1.0 - sigma))).astype(
        jnp.bfloat16
    )
    grad_upre = (grad_activ * swish).astype(jnp.bfloat16)
    grad_first = lax.dot_general(
        routed_rows, grad_gpre, contract_first, preferred_element_type=jnp.float32
    ).astype(jnp.bfloat16)
    grad_third = lax.dot_general(
        routed_rows, grad_upre, contract_first, preferred_element_type=jnp.float32
    ).astype(jnp.bfloat16)
    partial_value = lax.dot_general(
        grad_gpre, w_first, contract_last, preferred_element_type=jnp.float32
    ) + lax.dot_general(grad_upre, w_third, contract_last, preferred_element_type=jnp.float32)
    share = model_width // groups
    partial_groups = jnp.transpose(
        partial_value.astype(jnp.bfloat16).reshape(-1, groups, share), (1, 0, 2)
    )
    every_act, partial_groups = lax.optimization_barrier((every_act, partial_groups))
    home_rows = home_blocks(partial_groups.reshape(groups, experts, capacity, share))
    returned = lax.dot_general(
        full_table,
        home_rows.reshape(-1, share),
        contract_first,
        preferred_element_type=jnp.float32,
    )
    own_cotangent = lax.dynamic_slice_in_dim(
        cotangent, lax.axis_index("tp") * share, share, axis=1
    )
    mixer_share = (own_cotangent.astype(jnp.float32) + returned).astype(jnp.bfloat16)
    mixer_grad = lax.all_gather(mixer_share, "tp", axis=1, tiled=True)
    width_share = model_width // experts
    sent_columns = jnp.transpose(
        mixer_grad.reshape(tok_rows, experts, width_share), (1, 0, 2)
    )
    every_grad = lax.all_to_all(
        sent_columns, "sp", split_axis=0, concat_axis=0, tiled=True
    ).reshape(-1, width_share)
    grad_proj = lax.dot_general(
        every_grad, every_act, contract_first, preferred_element_type=jnp.float32
    )
    grad_act = lax.dot_general(
        mixer_grad, proj_weight, contract_last, preferred_element_type=jnp.float32
    )
    norm_output_gradient = (
        grad_act
        * gate_sig
        * (1.0 + normalized_values * (1.0 - gate_sig))
        * channel_norm_gain[None, :]
    )
    reduced_totals = lax.psum(
        (
            jnp.sum(norm_output_gradient, axis=1),
            jnp.sum(norm_output_gradient * normalized_input, axis=1),
        ),
        "tp",
    )
    channel_count = saved_normalized.shape[1] * groups
    conv_output_gradient = inverse_deviation[:, None] * (
        norm_output_gradient
        - reduced_totals[0][:, None] / channel_count
        - normalized_input * (reduced_totals[1][:, None] / channel_count)
    )
    reach = taps.shape[0] - 1
    beyond = from_behind(conv_output_gradient[:reach], "sp", -1)
    extended = jnp.concatenate([conv_output_gradient, beyond], axis=0)
    result = jnp.zeros_like(conv_output_gradient)
    for tap_index in range(taps.shape[0]):
        result = result + taps[tap_index][None, :] * extended[tap_index : tap_index + tok_rows]
    return (
        result.astype(jnp.bfloat16),
        grad_proj,
        grad_first[None],
        grad_third[None],
        grad_second[None],
    )


def solution(mesh):
    return jax.shard_map(
        shards,
        mesh=mesh,
        in_specs=(
            P("sp", None),
            P("sp", None),
            P("sp", None),
            P("sp", None),
            P("sp", "tp"),
            P("sp"),
            P("tp"),
            P(None, "tp"),
            P("tp", None),
            P("sp", None, "tp"),
            P("sp", None, "tp"),
            P("sp", "tp", None),
        ),
        out_specs=(
            P("sp", "tp"),
            P("sp", "tp"),
            P("sp", None, "tp"),
            P("sp", None, "tp"),
            P("sp", "tp", None),
        ),
        check_vma=False,
    )
```

profile of v0, /device:TPU:0, one launch (start us, length us, event | category | flops | bytes accessed | tf_op | source)
XLA Modules:
  0.0 155.1 jit_solution(12212289907834196503)
XLA Ops:
  7.2 1.0 copy.36
  8.5 0.6 reduce-window.6
  9.6 0.7 multiply_add_fusion
  10.6 1.3 convolution_convert_fusion.3
  12.0 1.6 %fusion.23 = bf16[128,512]{1,0:T(8,128)(2,1)} fusion(bf16[128,512]{1,0:T(8,128)(2,1)} %param.16, f32[512]{0:T(512)} %param.18), kind=kLoop, calls=%fused_computation.99 | loop fusion | flops 458752 | bytes 264192 | tf_op jit(solution)/shard_map/convert_element_type | solution.py:320
  13.6 0.9 fusion.119
  14.8 43.7 %shard_map.155 = (bf16[8,4,16,2048]{3,2,1,0:T(8,128)(2,1)S(1)}, bf16[8,4,16,2048]{3,2,1,0:T(8,128)(2,1)S(1)}) custom-call(bf16[8,16,2048]{2,1,0:T(8,128)(2,1)S(1)} %bitcast.103, bf16[8,16,2048]{2,1,0:T(8,128)(2,1)S(1)} %bitcast.104), custom_call_target="tpu_custom_call" | custom-call | bytes 41943040 | tf_op jit(solution)/shard_map/pallas_call | solution.py:149
  58.5 1.2 fusion.6
  59.8 1.8 %copy-done.6 = bf16[1,2048,512]{2,1,0:T(8,128)(2,1)S(1)} copy-done((bf16[1,2048,512]{2,1,0:T(8,128)(2,1)S(1)}, bf16[1,2048,512]{2,1,0:T(8,128)(2,1)}, u32[]{:S(2)}) %copy-start.6) | copy-done | bytes 2097176
  61.6 1.2 fusion.9
  62.9 0.7 copy-done.12
  63.6 1.6 %multiply_convert_fusion.1 = (bf16[512,512]{1,0:T(8,128)(2,1)S(1)}, bf16[512,512]{1,0:T(8,128)(2,1)S(1)}) fusion(f32[512,512]{1,0:T(8,128)S(1)} %fusion.6, f32[512,512]{1,0:T(8,128)S(1)} %fusion.9, bf16[512,2048]{1,0:T(8,128)(2,1)S(1)} %bitcast.105, bf16[1,512,2048]{2,1,0:T(8,128)(2,1)S(1)} %copy-done.12), kind=kOutput, calls=%fused_computation.55 | convolution fusion | flops 1077149696 | bytes 7340032 | tf_op jit(solution)/shard_map/dot_general | solution.py:342
  65.2 1.3 fusion.4
  66.5 1.3 add_convert_fusion
  67.8 1.5 copy.45
  69.7 0.7 fusion.125
  70.3 4.4 %fusion = bf16[1,2048,512]{2,1,0:T(8,128)(2,1)} fusion(bf16[512,2048]{1,0:T(8,128)(2,1)} %bitcast.109, bf16[512,512]{1,0:T(8,128)(2,1)S(1)} %get-tuple-element.22), kind=kOutput, calls=%fused_computation.33 | convolution fusion | flops 1074790400 | bytes 4718592 | tf_op jit(solution)/shard_map/dot_general | solution.py:349
  74.7 2.6 %fusion.1 = bf16[1,2048,512]{2,1,0:T(8,128)(2,1)} fusion(bf16[512,2048]{1,0:T(8,128)(2,1)S(1)} %bitcast.110, bf16[512,512]{1,0:T(8,128)(2,1)S(1)} %copy-done.9), kind=kOutput, calls=%fused_computation.34 | convolution fusion | flops 1074790400 | bytes 4718592 | tf_op jit(solution)/shard_map/dot_general | solution.py:352
  77.3 2.7 %fusion.2 = bf16[1,512,2048]{2,1,0:T(8,128)(2,1)} fusion(bf16[512,2048]{1,0:T(8,128)(2,1)S(1)} %bitcast.106, f32[512,512]{1,0:T(8,128)S(1)} %copy-done.16, f32[512,512]{1,0:T(8,128)S(1)} %copy-done.14), kind=kOutput, calls=%fused_computation.35 | convolution fusion | flops 1076363264 | bytes 6291456 | tf_op jit(solution)/shard_map/dot_general | solution.py:339
  80.1 1.6 %copy-done.1 = bf16[64,4,8,512]{3,2,0,1:T(8,128)(2,1)S(1)} copy-done((bf16[64,4,8,512]{3,2,0,1:T(8,128)(2,1)S(1)}, bf16[64,4,8,512]{3,2,0,1:T(8,128)(2,1)}, u32[]{:S(2)}) %copy-start.1) | copy-done | bytes 2097176
  81.6 31.1 %shard_map.156 = bf16[8,64,512]{2,1,0:T(8,128)(2,1)S(1)} custom-call(bf16[4,8,64,512]{3,2,1,0:T(8,128)(2,1)S(1)} %bitcast.101), custom_call_target="tpu_custom_call" | custom-call | bytes 41943040 | tf_op jit(solution)/shard_map/pallas_call | solution.py:268
  113.1 6.5 %all_gather.7 = bf16[128,2048]{1,0:T(8,128)(2,1)S(1)} all-gather(bf16[128,512]{1,0:T(8,128)(2,1)S(1)} %fusion.15), channel_id=1, replica_groups=mesh['sp'=8,'tp'=4] {'tp'}, dimensions={1}, use_global_device_ids=true | all-gather | bytes 655360 | tf_op jit(solution)/shard_map/all_gather | solution.py:374
  119.6 0.8 copy.46
  120.4 5.7 %all-to-all-start = ((bf16[8,128,256]{2,1,0:T(8,128)(2,1)}), bf16[8,128,256]{2,1,0:T(8,128)(2,1)S(1)}, u32[]{:S(2)}, u32[]{:S(2)}) async-start(bf16[8,128,256]{2,1,0:T(8,128)(2,1)} %bitcast.100), calls=%async_computation | async-start | bytes 1048576 | tf_op jit(solution)/shard_map/all_to_all | solution.py:379
  126.1 3.1 %fusion.124 = (f32[128]{0:T(128)}, f32[128]{0:T(128)}, f32[128,512]{1,0:T(8,128)S(1)}) fusion(bf16[128,512]{1,0:T(8,128)(2,1)S(1)} %copy-done.10, f32[512]{0:T(512)} %param.18, bf16[128,2048]{1,0:T(8,128)(2,1)S(1)} %all_gather.7, bf16[512,2048]{1,0:T(8,128)(2,1)} %param.20), kind=kOutput, calls=%fused_computation.213 | convolution fusion | flops 269352704 | bytes 3017728 | tf_op jit(solution)/shard_map/dot_general | solution.py:385
  129.2 6.9 %all-reduce = (f32[128]{0:T(128)S(1)}, f32[128]{0:T(128)S(1)}) all-reduce(f32[128]{0:T(128)} %get-tuple-element.18, f32[128]{0:T(128)} %get-tuple-element.17), channel_id=1, replica_groups=mesh['sp'=8,'tp'=4] {'tp'}, use_global_device_ids=true, to_apply=%region_9.10 | all-reduce | flops 256 | bytes 2048 | tf_op jit(solution)/shard_map/psum | solution.py:394
  136.1 0.8 fusion.27
  136.9 1.3 collective-permute-start
  138.2 1.0 fusion.126
  139.3 3.8 %collective-permute-done = f32[30,512]{1,0:T(8,128)S(1)} collective-permute-done((f32[30,512]{1,0:T(8,128)S(1)}, f32[30,512]{1,0:T(8,128)S(1)}, u32[]{:S(2)}, u32[]{:S(2)}) %collective-permute-start) | collective-permute-done | bytes 61472 | tf_op jit(solution)/shard_map/ppermute | solution.py:14
  143.1 2.7 %fusion.32 = bf16[128,512]{1,0:T(8,128)(2,1)} fusion(f32[128,512]{1,0:T(8,128)S(1)} %fusion.27, f32[30,512]{1,0:T(8,128)S(1)} %collective-permute-done, f32[512]{0:T(512)S(1)} %bitcast.143, f32[512]{0:T(512)S(1)} %bitcast.144, f32[512]{0:T(512)S(1)} %bitcast.115, f32[512]{0:T(512)S(1)} %bitcast.116, f32[512]{0:T(512)S(1)} %bitcast.117, f32[512]{0:T(512)} %bitcast.118, ...), kind=kLoop, calls=%fused_computation.108 | loop fusion | flops 6029312 | bytes 518144 | tf_op jit(solution)/shard_map/convert_element_type | solution.py:414
  145.8 2.5 %fusion.127 = f32[256,512]{1,0:T(8,128)} fusion(bf16[1024,256]{1,0:T(8,128)(2,1)S(1)} %bitcast.113, bf16[1024,512]{1,0:T(8,128)(2,1)} %all-gather.2.cloned.1.call-done), kind=kOutput, calls=%fused_computation.216 | convolution fusion | flops 268435456 | bytes 2097152 | tf_op jit(solution)/shard_map/dot_general | solution.py:382
  (56 shorter events, 2.1 us)
Async XLA Ops:
  7.2 51.3 %copy-start = (bf16[1,2048,512]{2,1,0:T(8,128)(2,1)S(1)}, bf16[1,2048,512]{2,1,0:T(8,128)(2,1)}, u32[]{:S(2)}) copy-start(bf16[1,2048,512]{2,1,0:T(8,128)(2,1)} %param.21) | copy-start | bytes 6291460
  7.2 7.3 %copy-start.7 = (bf16[128,2048]{1,0:T(8,128)(2,1)S(1)}, bf16[128,2048]{1,0:T(8,128)(2,1)}, u32[]{:S(2)}) copy-start(bf16[128,2048]{1,0:T(8,128)(2,1)} %param.12) | copy-start | bytes 1572868
  7.2 72.9 %all-gather.2.cloned.1.call-start = ((), (), s32[]{:S(2)}) async-start(), calls=%async_computation.1 | async-start | bytes 1179648 | tf_op jit(solution)/shard_map/all_gather | solution.py:322
  58.5 1.3 copy-start.4
  58.5 4.4 %copy-start.2 = (bf16[8,4,16,2048]{3,2,1,0:T(8,128)(2,1)}, bf16[8,4,16,2048]{3,2,1,0:T(8,128)(2,1)S(1)}, u32[]{:S(2)}) copy-start(bf16[8,4,16,2048]{3,2,1,0:T(8,128)(2,1)S(1)} %get-tuple-element.13) | copy-start | bytes 6291460
  58.5 3.1 %copy-start.6 = (bf16[1,2048,512]{2,1,0:T(8,128)(2,1)S(1)}, bf16[1,2048,512]{2,1,0:T(8,128)(2,1)}, u32[]{:S(2)}) copy-start(bf16[1,2048,512]{2,1,0:T(8,128)(2,1)} %param.22) | copy-start | bytes 6291460
  61.6 1.3 copy-start.13
  61.6 2.0 %copy-start.12 = (bf16[1,512,2048]{2,1,0:T(8,128)(2,1)S(1)}, bf16[1,512,2048]{2,1,0:T(8,128)(2,1)}, u32[]{:S(2)}) copy-start(bf16[1,512,2048]{2,1,0:T(8,128)(2,1)} %param.23) | copy-start | bytes 6291460
  62.9 2.3 %copy-start.15 = (f32[512,512]{1,0:T(8,128)}, f32[512,512]{1,0:T(8,128)S(1)}, u32[]{:S(2)}) copy-start(f32[512,512]{1,0:T(8,128)S(1)} %fusion.9) | copy-start | bytes 3145732
  65.2 1.3 copy-start.8
  67.8 1.9 %copy-start.11 = (f32[31,512]{1,0:T(8,128)S(1)}, f32[31,512]{1,0:T(8,128)}, u32[]{:S(2)}) copy-start(f32[31,512]{1,0:T(8,128)} %param.19) | copy-start | bytes 190468
  70.3 4.4 %copy-start.5 = (bf16[8,4,16,2048]{3,2,1,0:T(8,128)(2,1)S(1)}, bf16[8,4,16,2048]{3,2,1,0:T(8,128)(2,1)}, u32[]{:S(2)}) copy-start(bf16[8,4,16,2048]{3,2,1,0:T(8,128)(2,1)} %copy-done.4) | copy-start | bytes 6291460
  70.3 4.4 %copy-start.9 = (bf16[512,512]{1,0:T(8,128)(2,1)S(1)}, bf16[512,512]{1,0:T(8,128)(2,1)}, u32[]{:S(2)}) copy-start(bf16[512,512]{1,0:T(8,128)(2,1)} %copy-done.8) | copy-start | bytes 1572868
  74.7 2.6 %copy-start.3 = (bf16[8,4,16,2048]{3,2,1,0:T(8,128)(2,1)S(1)}, bf16[8,4,16,2048]{3,2,1,0:T(8,128)(2,1)}, u32[]{:S(2)}) copy-start(bf16[8,4,16,2048]{3,2,1,0:T(8,128)(2,1)} %copy-done.2) | copy-start | bytes 6291460
  74.7 2.6 %copy-start.14 = (f32[512,512]{1,0:T(8,128)S(1)}, f32[512,512]{1,0:T(8,128)}, u32[]{:S(2)}) copy-start(f32[512,512]{1,0:T(8,128)} %copy-done.13) | copy-start | bytes 3145732
  74.7 2.6 %copy-start.16 = (f32[512,512]{1,0:T(8,128)S(1)}, f32[512,512]{1,0:T(8,128)}, u32[]{:S(2)}) copy-start(f32[512,512]{1,0:T(8,128)} %copy-done.15) | copy-start | bytes 3145732
  80.1 1.6 %copy-start.1 = (bf16[64,4,8,512]{3,2,0,1:T(8,128)(2,1)S(1)}, bf16[64,4,8,512]{3,2,0,1:T(8,128)(2,1)}, u32[]{:S(2)}) copy-start(bf16[64,4,8,512]{3,2,0,1:T(8,128)(2,1)} %copy.45) | copy-start | bytes 6291460
  112.8 13.3 %copy-start.10 = (bf16[128,512]{1,0:T(8,128)(2,1)S(1)}, bf16[128,512]{1,0:T(8,128)(2,1)}, u32[]{:S(2)}) copy-start(bf16[128,512]{1,0:T(8,128)(2,1)} %param.16) | copy-start | bytes 393220
  120.4 25.4 %all-to-all-start = ((bf16[8,128,256]{2,1,0:T(8,128)(2,1)}), bf16[8,128,256]{2,1,0:T(8,128)(2,1)S(1)}, u32[]{:S(2)}, u32[]{:S(2)}) async-start(bf16[8,128,256]{2,1,0:T(8,128)(2,1)} %bitcast.100), calls=%async_computation | async-start | bytes 1048576 | tf_op jit(solution)/shard_map/all_to_all | solution.py:379
  136.9 6.2 %collective-permute-start = (f32[30,512]{1,0:T(8,128)S(1)}, f32[30,512]{1,0:T(8,128)S(1)}, u32[]{:S(2)}, u32[]{:S(2)}) collective-permute-start(f32[30,512]{1,0:T(8,128)S(1)} %slice.257), channel_id=1, source_target_pairs={{4,0},{8,4},{12,8},{16,12},{20,16},{24,20},{28,24},{5,1},{9,5},{13... | collective-permute-start | bytes 184328 | tf_op jit(solution)/shard_map/ppermute | solution.py:14
Sparse Core Ops, SparseCore 0:
  13.7 50.6 all-gather.1
where the time goes:
time: 156 us; the launch traced here: 155 us
  Pallas kernels  74.8 us (48%)
  matrix products  23.8 us (15%)
  between operations  14.3 us (9%)
  blocking collectives  13.4 us (9%)
  local copies, waits for them, and re-layouts  10.1 us (6%)
  other arithmetic  7.78 us (5%)
  starting transfers between devices  7 us (4%)
  waiting for transfers between devices  3.84 us (2%)
    pallas_call x1, Pallas kernels, dispatch_blocks(): pl.pallas_call(functools.partial(dispatch_kernel, experts, groups), out_s...  43.7 us
    pallas_call x1, Pallas kernels, home_blocks(): pl.pallas_call(functools.partial(home_kernel, experts, groups), out_shape...  31.1 us
    psum x1, blocking collectives, shards(): lax.psum((jnp.sum(norm_output_gradient, axis=1), jnp.sum(norm_output_grad...  6.92 us
    all_gather x1, blocking collectives, shards(): mixer_grad = lax.all_gather(mixer_share, 'tp', axis=1, tiled=True)  6.5 us
    all_to_all x1, starting transfers between devices, shards(): lax.all_to_all(sent_columns, 'sp', split_axis=0, concat_axis=0, tiled=True)  5.67 us
    unnamed x35, local copies, waits for them, and re-layouts  5.16 us
    dot_general x1, matrix products, shards(): lax.dot_general(routed_rows, grad_gpre, contract_first, preferred_element...  4.35 us
    ppermute x1, waiting for transfers between devices, from_behind(): lax.ppermute(value, axis, [(source, source + steps) for source in range(l...  3.82 us
  transfers between devices with their start and end apart: 3, of which 1 were waited for; matrix products, arithmetic and copies ran while one was open for 18% of the time, Pallas kernels for 28%

commit v1 on v0

--- a/solution.py
+++ b/solution.py
@@ -6,12 +6,6 @@
 from jax.experimental import pallas as pl
 from jax.experimental.pallas import tpu as pltpu
 from jax.sharding import PartitionSpec as P
-
-
-def from_behind(value, axis, steps):
-    count = lax.axis_size(axis)
-    leading, last = (max(0, -steps), min(count, count - steps))
-    return lax.ppermute(value, axis, [(source, source + steps) for source in range(leading, last)])
 
 
 def route_table(expert_ids, route_weight, slot_start, slot_span, capacity, experts):
@@ -281,6 +275,283 @@
             flops=0, bytes_accessed=40 * partial.size, transcendentals=0
         ),
     )(partial)
+
+
+def line_width(experts):
+    width = 1
+    while 4 * width * width <= experts and experts % (2 * width) == 0:
+        width = 2 * width
+    return width
+
+
+def sigmoid(value):
+    return 1.0 / (1.0 + jnp.exp(-value))
+
+
+def tail_kernel(
+    experts, groups, lead, table, home, cotangent, saved, inverse, gain, taps, weight, result,
+    grad_proj, blocks, every, acts, sums, extended, *sems
+):
+    (row_send, row_recv, pair_send, pair_recv, far_send, far_recv, half_send, half_recv,
+     line_send, line_recv, side_send, side_recv, sum_send, sum_recv, halo_send, halo_recv) = sems
+    mine = lax.axis_index("sp")
+    place = lax.axis_index("tp")
+    chips = groups // 2
+    chip, core = place // 2, place % 2
+    sibling = chip * 2 + 1 - core
+    across = experts // lead
+    line, side = mine // lead, mine % lead
+    tok = saved.shape[0]
+    channels = saved.shape[1]
+    width = blocks.shape[-1]
+    per = experts // groups
+    half = tok // 2
+
+    def at_chip(step):
+        return ((chip + step) % chips) * 2 + core
+
+    barrier = pltpu.get_barrier_semaphore()
+
+    def greet(step, carry):
+        pl.semaphore_signal(barrier, inc=1, device_id=((mine + step) % experts, place),
+                            device_id_type=pl.DeviceIdType.MESH)
+        return carry
+
+    def greet_group(step, carry):
+        pl.semaphore_signal(barrier, inc=1, device_id=(mine, (place + step) % groups),
+                            device_id_type=pl.DeviceIdType.MESH)
+        return carry
+
+    lax.fori_loop(1, experts, greet, 0)
+    lax.fori_loop(1, groups, greet_group, 0)
+    normalized = saved[...].astype(jnp.float32)
+    scaled = normalized * gain[...]
+    gate = sigmoid(scaled)
+    acts[mine] = (scaled * gate).astype(jnp.bfloat16)
+    pl.semaphore_wait(barrier, experts + groups - 2)
+
+    def along(step):
+        return remote(acts.at[mine], acts.at[mine], line_send.at[step], line_recv.at[step],
+                      (((line + step) % across) * lead + side, place))
+
+    def arrived(step):
+        source = ((line + across - step) % across) * lead + side
+        return remote(acts.at[source], acts.at[source], line_send.at[step], line_recv.at[step],
+                      (((line + step) % across) * lead + side, place))
+
+    def beside(step, hop):
+        source = ((line + across - step) % across) * lead + side
+        return remote(acts.at[source], acts.at[source], side_send.at[step, hop],
+                      side_recv.at[step, hop], (line * lead + (side + hop) % lead, place))
+
+    def share_at(owner):
+        return blocks.at[pl.ds(owner * per, per)]
+
+    def row(hop):
+        return remote(share_at(place), share_at(place), row_send.at[hop], row_recv.at[hop],
+                      (mine, at_chip(hop)))
+
+    def pair(hop):
+        owner = at_chip(chips - hop)
+        return remote(share_at(owner), share_at(owner), pair_send.at[hop], pair_recv.at[hop],
+                      (mine, sibling))
+
+    share = jnp.dot(table[...], home[...], preferred_element_type=jnp.float32)
+    share = (share + cotangent[...].astype(jnp.float32)).astype(jnp.bfloat16)
+    for part in range(per):
+        piece = share[:, part * width : (part + 1) * width]
+        blocks[place * per + part] = piece.reshape(2, half, width)
+    for hop in range(1, chips):
+        row(hop).start()
+    pair(0).start()
+    for step in range(1, across):
+        along(step).start()
+    for hop in range(1, lead):
+        beside(0, hop).start()
+    for hop in range(1, chips):
+        row(hop).wait_recv()
+        pair(hop).start()
+    for hop in range(chips):
+        pair(hop).wait_recv()
+
+    def far(step):
+        peer = (mine + step) % experts
+        return remote(blocks.at[peer, core], every.at[mine, core], far_send.at[step],
+                      far_recv.at[step], (peer, place))
+
+    def to_half(step):
+        source = (mine + experts - step) % experts
+        return remote(every.at[source, core], every.at[source, core], half_send.at[step],
+                      half_recv.at[step], (mine, sibling))
+
+    def start_far(step, carry):
+        far(step).start()
+        return carry
+
+    lax.fori_loop(1, experts, start_far, 0)
+    every[mine] = blocks[mine]
+
+    grad = jnp.zeros((tok, channels), jnp.float32)
+    for part in range(experts):
+        grad = grad + lax.dot_general(
+            blocks[part].reshape(tok, width),
+            weight[:, part * width : (part + 1) * width],
+            (((1,), (1,)), ((), ())),
+            preferred_element_type=jnp.float32,
+        )
+    normalized = saved[...].astype(jnp.float32)
+    scaled = normalized * gain[...]
+    gate = sigmoid(scaled)
+    grad = grad * gate * (1.0 + scaled * (1.0 - gate)) * gain[...]
+    lanes = min(channels, 128)
+    first = jnp.zeros((tok, lanes), jnp.float32)
+    second = jnp.zeros((tok, lanes), jnp.float32)
+    for at in range(0, channels, lanes):
+        first = first + grad[:, at : at + lanes]
+        second = second + grad[:, at : at + lanes] * normalized[:, at : at + lanes]
+    sums[place, 0] = jnp.sum(jnp.transpose(first).reshape(lanes // 8, 8, tok), axis=0)
+    sums[place, 1] = jnp.sum(jnp.transpose(second).reshape(lanes // 8, 8, tok), axis=0)
+
+    def tell(step):
+        return remote(sums.at[place], sums.at[place], sum_send.at[step], sum_recv.at[step],
+                      (mine, (place + step) % groups))
+
+    def start_tell(step, carry):
+        tell(step).start()
+        return carry
+
+    def wait_tell(step, carry):
+        tell(step).wait()
+        return carry
+
+    lax.fori_loop(1, groups, start_tell, 0)
+    for step in range(1, across - 1):
+        arrived(step).wait_recv()
+        for hop in range(1, lead):
+            beside(step, hop).start()
+    lax.fori_loop(1, groups, wait_tell, 0)
+    count = channels * groups
+    total = jnp.sum(sums[...], axis=0)
+
+    def column(kind):
+        flat = jnp.sum(total[kind], axis=0, keepdims=True) / count
+        return jnp.transpose(jnp.broadcast_to(flat, (lanes, tok)))
+
+    mean, slope = column(0), column(1)
+    for at in range(0, channels, lanes):
+        extended[at // lanes, 0:tok] = inverse[...] * (
+            grad[:, at : at + lanes] - mean - normalized[:, at : at + lanes] * slope
+        )
+    reach = extended.shape[1] - tok
+
+    def halo():
+        return remote(extended.at[:, pl.ds(0, reach)], extended.at[:, pl.ds(tok, reach)],
+                      halo_send, halo_recv, ((mine + experts - 1) % experts, place))
+
+    @pl.when(mine > 0)
+    def _():
+        halo().start()
+
+    @pl.when(mine == experts - 1)
+    def _():
+        extended[:, tok : tok + reach] = jnp.zeros((channels // lanes, reach, lanes), jnp.float32)
+
+    arrived(across - 1).wait_recv()
+    for hop in range(1, lead):
+        beside(across - 1, hop).start()
+
+    def forward(step, carry):
+        far(step).wait_recv()
+        to_half(step).start()
+        return carry
+
+    lax.fori_loop(1, experts, forward, 0)
+
+    @pl.when(mine < experts - 1)
+    def _():
+        halo().wait_recv()
+
+    for at in range(0, channels, lanes):
+        value = jnp.zeros((tok, lanes), jnp.float32)
+        for tap in range(taps.shape[0]):
+            value = value + taps[tap : tap + 1, at : at + lanes] * extended[at // lanes, tap : tap + tok]
+        result[:, at : at + lanes] = value.astype(result.dtype)
+
+    def arrive(step, carry):
+        to_half(step).wait_recv()
+        return carry
+
+    lax.fori_loop(1, experts, arrive, 0)
+    for step in range(across):
+        for hop in range(1, lead):
+            beside(step, hop).wait_recv()
+    grad_proj[...] = lax.dot_general(
+        every[...].reshape(experts * tok, width),
+        acts[...].reshape(experts * tok, channels),
+        (((0,), (0,)), ((), ())),
+        preferred_element_type=jnp.float32,
+    )
+
+    @pl.when(mine > 0)
+    def _():
+        halo().wait_send()
+
+    for hop in range(chips):
+        pair(hop).wait_send()
+        if hop:
+            row(hop).wait_send()
+    for step in range(across):
+        if step:
+            along(step).wait_send()
+        for hop in range(1, lead):
+            beside(step, hop).wait_send()
+
+    def finish(step, carry):
+        far(step).wait_send()
+        to_half(step).wait_send()
+        return carry
+
+    lax.fori_loop(1, experts, finish, 0)
+
+
+def tail_blocks(table, home, cotangent, saved, inverse, gain, taps, weight, experts, groups):
+    tok, channels = saved.shape
+    model_width = weight.shape[1]
+    width = model_width // experts
+    lead = line_width(experts)
+    across = experts // lead
+    lanes = min(channels, 128)
+    reach = (taps.shape[0] + 6) // 8 * 8
+    dma = pltpu.SemaphoreType.DMA
+    vmem = pl.BlockSpec(memory_space=pltpu.VMEM)
+    return pl.pallas_call(
+        functools.partial(tail_kernel, experts, groups, lead),
+        out_shape=(
+            jax.ShapeDtypeStruct((tok, channels), jnp.bfloat16),
+            jax.ShapeDtypeStruct((width, channels), jnp.float32),
+        ),
+        in_specs=[vmem] * 8,
+        out_specs=[vmem] * 2,
+        scratch_shapes=[
+            pltpu.VMEM((experts, 2, tok // 2, width), jnp.bfloat16),
+            pltpu.VMEM((experts, 2, tok // 2, width), jnp.bfloat16),
+            pltpu.VMEM((experts, tok, channels), jnp.bfloat16),
+            pltpu.VMEM((groups, 2, 8, tok), jnp.float32),
+            pltpu.VMEM((channels // lanes, tok + reach, lanes), jnp.float32),
+        ]
+        + [dma((groups // 2,))] * 4
+        + [dma((experts,))] * 4
+        + [dma((across,))] * 2
+        + [dma((across, lead))] * 2
+        + [dma((groups,))] * 2
+        + [dma] * 2,
+        compiler_params=pltpu.CompilerParams(
+            collective_id=2, has_side_effects=True, vmem_limit_bytes=32 * 2**20
+        ),
+        cost_estimate=pl.CostEstimate(
+            flops=10**9, bytes_accessed=10**7, transcendentals=0
+        ),
+    )(table, home, cotangent, saved, inverse, gain, taps, weight)
 
 
 def shards(
@@ -314,12 +585,6 @@
     ).astype(jnp.bfloat16)
     sent_rows = sent_rows.reshape(experts, slot_span, model_width)
     sent_grad = sent_grad.reshape(experts, slot_span, model_width)
-    normalized_input = saved_normalized.astype(jnp.float32)
-    normalized_values = normalized_input * channel_norm_gain[None, :]
-    gate_sig = jax.nn.sigmoid(normalized_values)
-    act_conv = (normalized_values * gate_sig).astype(jnp.bfloat16)
-    act_conv, sent_rows = lax.optimization_barrier((act_conv, sent_rows))
-    every_act = lax.all_gather(act_conv, "sp", axis=0, tiled=True)
     routed_rows, routed_grad = dispatch_blocks(sent_rows, sent_grad, groups)
     full_table, unused_weight = route_table(
         expert_ids, route_weight, 0, capacity, capacity, experts
@@ -359,59 +624,24 @@
     partial_groups = jnp.transpose(
         partial_value.astype(jnp.bfloat16).reshape(-1, groups, share), (1, 0, 2)
     )
-    every_act, partial_groups = lax.optimization_barrier((every_act, partial_groups))
     home_rows = home_blocks(partial_groups.reshape(groups, experts, capacity, share))
-    returned = lax.dot_general(
-        full_table,
-        home_rows.reshape(-1, share),
-        contract_first,
-        preferred_element_type=jnp.float32,
-    )
     own_cotangent = lax.dynamic_slice_in_dim(
         cotangent, lax.axis_index("tp") * share, share, axis=1
     )
-    mixer_share = (own_cotangent.astype(jnp.float32) + returned).astype(jnp.bfloat16)
-    mixer_grad = lax.all_gather(mixer_share, "tp", axis=1, tiled=True)
-    width_share = model_width // experts
-    sent_columns = jnp.transpose(
-        mixer_grad.reshape(tok_rows, experts, width_share), (1, 0, 2)
-    )
-    every_grad = lax.all_to_all(
-        sent_columns, "sp", split_axis=0, concat_axis=0, tiled=True
-    ).reshape(-1, width_share)
-    grad_proj = lax.dot_general(
-        every_grad, every_act, contract_first, preferred_element_type=jnp.float32
-    )
-    grad_act = lax.dot_general(
-        mixer_grad, proj_weight, contract_last, preferred_element_type=jnp.float32
-    )
-    norm_output_gradient = (
-        grad_act
-        * gate_sig
-        * (1.0 + normalized_values * (1.0 - gate_sig))
-        * channel_norm_gain[None, :]
-    )
-    reduced_totals = lax.psum(
-        (
-            jnp.sum(norm_output_gradient, axis=1),
-            jnp.sum(norm_output_gradient * normalized_input, axis=1),
-        ),
-        "tp",
-    )
-    channel_count = saved_normalized.shape[1] * groups
-    conv_output_gradient = inverse_deviation[:, None] * (
-        norm_output_gradient
-        - reduced_totals[0][:, None] / channel_count
-        - normalized_input * (reduced_totals[1][:, None] / channel_count)
-    )
-    reach = taps.shape[0] - 1
-    beyond = from_behind(conv_output_gradient[:reach], "sp", -1)
-    extended = jnp.concatenate([conv_output_gradient, beyond], axis=0)
-    result = jnp.zeros_like(conv_output_gradient)
-    for tap_index in range(taps.shape[0]):
-        result = result + taps[tap_index][None, :] * extended[tap_index : tap_index + tok_rows]
+    result, grad_proj = tail_blocks(
+        jnp.transpose(full_table),
+        home_rows.reshape(-1, share),
+        own_cotangent,
+        saved_normalized,
+        inverse_deviation[:, None],
+        channel_norm_gain[None, :],
+        taps,
+        proj_weight,
+        experts,
+        groups,
+    )
     return (
-        result.astype(jnp.bfloat16),
+        result,
         grad_proj,
         grad_first[None],
         grad_third[None],

time: 156 us -> 124 us (0.79)
  Pallas kernels: 74.8 us -> 95.5 us
  blocking collectives: 13.4 us -> 0 us
  between operations: 14.3 us -> 0.94 us
  starting transfers between devices: 7 us -> 0 us
  matrix products: 23.8 us -> 17.2 us
  other arithmetic: 7.78 us -> 2.67 us
  waiting for transfers between devices: 3.84 us -> 0 us
  local copies, waits for them, and re-layouts: 10.1 us -> 7.37 us
    pallas_call x0 -> x1, Pallas kernels: none -> 25 us  [tail_blocks(): pl.pallas_call(functools.partial(tail_kernel, experts, groups, lead), out...]
    psum x1 -> x0, blocking collectives: 6.92 us -> none  [shards(): lax.psum((jnp.sum(norm_output_gradient, axis=1), jnp.sum(norm_output_grad...]
    all_gather x1 -> x0, blocking collectives: 6.5 us -> none  [shards(): mixer_grad = lax.all_gather(mixer_share, 'tp', axis=1, tiled=True)]
    dot_general x3 -> x0, matrix products: 5.88 us -> none  [the longest x1 3.12 us: shards(): lax.dot_general(mixer_grad, proj_weight, contract_last, preferred_element...]
    all_to_all x1 -> x0, starting transfers between devices: 5.67 us -> none  [shards(): lax.all_to_all(sent_columns, 'sp', split_axis=0, concat_axis=0, tiled=True)]
    convert_element_type x2 -> x1, other arithmetic: 4.35 us -> 0.01 us  [route_table(): dispatch = jnp.any(matched, axis=2).astype(jnp.bfloat16)]
    ppermute x1 -> x0, waiting for transfers between devices: 3.82 us -> none  [from_behind(): lax.ppermute(value, axis, [(source, source + steps) for source in range(l...]
    pallas_call x1, Pallas kernels: 31.1 us -> 28.9 us  [home_blocks(): pl.pallas_call(functools.partial(home_kernel, experts, groups), out_shape...]
  transfers between devices with their start and end apart: 3 -> 0, of which waited for: 1 -> 0; matrix products, arithmetic and copies ran while one was open for 18% -> 0% of each run, Pallas kernels for 28% -> 0%
where the time goes in v1:
time: 124 us
  Pallas kernels  95.5 us (77%)
  matrix products  17.2 us (14%)
  local copies, waits for them, and re-layouts  7.37 us (6%)
  other arithmetic  2.67 us (2%)
    pallas_call x1, Pallas kernels, dispatch_blocks(): pl.pallas_call(functools.partial(dispatch_kernel, experts, groups), out_s...  41.6 us
    pallas_call x1, Pallas kernels, home_blocks(): pl.pallas_call(functools.partial(home_kernel, experts, groups), out_shape...  28.9 us
    pallas_call x1, Pallas kernels, tail_blocks(): pl.pallas_call(functools.partial(tail_kernel, experts, groups, lead), out...  25 us
    unnamed x31, local copies, waits for them, and re-layouts  5.13 us
    dot_general x1, matrix products, shards(): lax.dot_general(activ, routed_grad, contract_first, preferred_element_typ...  2.68 us
    dot_general x1, matrix products, shards(): lax.dot_general(routed_rows, grad_gpre, contract_first, preferred_element...  2.62 us
    dot_general x1, matrix products, shards(): lax.dot_general(routed_rows, grad_upre, contract_first, preferred_element...  2.61 us

profile of v1, /device:TPU:0, one launch (start us, length us, event | category | flops | bytes accessed | tf_op | source)
XLA Modules:
  0.0 123.7 jit_solution(3713400854080545340)
XLA Ops:
  0.6 0.9 copy.38
  1.6 0.1 eq.63
  1.7 0.6 reduce-window.6
  2.3 0.2 slice_reduce_fusion
  2.6 0.1 eq.59
  2.7 0.1 fusion.17
  2.8 0.1 reshape.94
  3.0 0.7 multiply_add_fusion
  3.9 0.1 compare_reduce_fusion.1
  4.0 0.9 fusion.15
  4.8 1.3 %fusion.3 = bf16[128,2048]{1,0:T(8,128)(2,1)S(1)} fusion(pred[128,128]{1,0:T(8,128)(4,1)S(1)} %compare_reduce_fusion.1, bf16[128,2048]{1,0:T(8,128)(2,1)} %param.12, f32[128]{0:T(128)S(1)} %fusion.15), kind=kOutput, calls=%fused_computation.8 | convolution fusion | flops 67633152 | bytes 1065472 | tf_op jit(solution)/shard_map/dot_general | solution.py:584
  6.2 1.3 %convolution_convert_fusion.3 = bf16[128,2048]{1,0:T(8,128)(2,1)S(1)} fusion(pred[128,128]{1,0:T(8,128)(4,1)S(1)} %compare_reduce_fusion.1, bf16[128,2048]{1,0:T(8,128)(2,1)} %param.13), kind=kOutput, calls=%fused_computation.9 | convolution fusion | flops 67371008 | bytes 1064960 | tf_op jit(solution)/shard_map/dot_general | solution.py:580
  7.5 41.6 %shard_map.155 = (bf16[8,4,16,2048]{3,2,1,0:T(8,128)(2,1)S(1)}, bf16[8,4,16,2048]{3,2,1,0:T(8,128)(2,1)S(1)}) custom-call(bf16[8,16,2048]{2,1,0:T(8,128)(2,1)S(1)} %bitcast.61, bf16[8,16,2048]{2,1,0:T(8,128)(2,1)S(1)} %bitcast.60), custom_call_target="tpu_custom_call" | custom-call | bytes 41943040 | tf_op jit(solution)/shard_map/pallas_call | solution.py:143
  49.2 1.2 %fusion.6 = f32[512,512]{1,0:T(8,128)S(1)} fusion(bf16[512,2048]{1,0:T(8,128)(2,1)S(1)} %bitcast.63, bf16[1,2048,512]{2,1,0:T(8,128)(2,1)S(1)} %copy-done), kind=kOutput, calls=%fused_computation.13 | convolution fusion | flops 1073741824 | bytes 5242880 | tf_op jit(solution)/shard_map/dot_general | solution.py:599
  50.5 1.0 copy-done.7
  51.5 1.2 %fusion.9 = f32[512,512]{1,0:T(8,128)S(1)} fusion(bf16[512,2048]{1,0:T(8,128)(2,1)S(1)} %bitcast.64, bf16[1,2048,512]{2,1,0:T(8,128)(2,1)S(1)} %copy-done.7), kind=kOutput, calls=%fused_computation.16 | convolution fusion | flops 1073741824 | bytes 5242880 | tf_op jit(solution)/shard_map/dot_general | solution.py:600
  52.8 2.7 %fusion.2 = bf16[1,512,2048]{2,1,0:T(8,128)(2,1)} fusion(bf16[512,2048]{1,0:T(8,128)(2,1)S(1)} %bitcast.67, f32[512,512]{1,0:T(8,128)S(1)} %fusion.9, f32[512,512]{1,0:T(8,128)S(1)} %fusion.6), kind=kOutput, calls=%fused_computation.6 | convolution fusion | flops 1076363264 | bytes 6291456 | tf_op jit(solution)/shard_map/dot_general | solution.py:604
  55.5 1.6 %multiply_convert_fusion.1 = (bf16[512,512]{1,0:T(8,128)(2,1)S(1)}, bf16[512,512]{1,0:T(8,128)(2,1)S(1)}) fusion(f32[512,512]{1,0:T(8,128)S(1)} %fusion.6, f32[512,512]{1,0:T(8,128)S(1)} %fusion.9, bf16[512,2048]{1,0:T(8,128)(2,1)S(1)} %bitcast.68, bf16[1,512,2048]{2,1,0:T(8,128)(2,1)S(1)} %copy-done.13), kind=kOutput, calls=%fused_computation.21 | convolution fusion | flops 1077149696 | bytes 7340032 | tf_op jit(solution)/shard_map/dot_general | solution.py:607
  57.1 1.3 %fusion.4 = f32[512,2048]{1,0:T(8,128)S(1)} fusion(bf16[512,512]{1,0:T(8,128)(2,1)S(1)} %get-tuple-element.14, bf16[1,2048,512]{2,1,0:T(8,128)(2,1)S(1)} %copy-done), kind=kOutput, calls=%fused_computation.11 | convolution fusion | flops 1073741824 | bytes 6815744 | tf_op jit(solution)/shard_map/dot_general | solution.py:620
  58.4 1.3 %add_convert_fusion = bf16[512,2048]{1,0:T(8,128)(2,1)S(1)} fusion(f32[512,2048]{1,0:T(8,128)S(1)} %fusion.4, bf16[512,512]{1,0:T(8,128)(2,1)S(1)} %get-tuple-element.13, bf16[1,2048,512]{2,1,0:T(8,128)(2,1)S(1)} %copy-done.7), kind=kOutput, calls=%fused_computation | convolution fusion | flops 1075838976 | bytes 8912896 | tf_op jit(solution)/shard_map/dot_general | solution.py:622
  59.7 0.2 copy.46
  59.9 28.9 %shard_map.156 = bf16[8,64,512]{2,1,0:T(8,128)(2,1)S(1)} custom-call(bf16[4,8,64,512]{3,2,1,0:T(8,128)(2,1)S(1)} %bitcast.59), custom_call_target="tpu_custom_call" | custom-call | bytes 41943040 | tf_op jit(solution)/shard_map/pallas_call | solution.py:262
  88.9 0.9 constant_dynamic-slice_fusion.cotangent
  90.0 0.1 compare_reduce_fusion
  90.1 0.2 copy.41
  90.3 0.1 copy.43.inverse
  90.5 1.6 %copy-done.1 = bf16[512,2048]{1,0:T(8,128)(2,1)S(1)} copy-done((bf16[512,2048]{1,0:T(8,128)(2,1)S(1)}, bf16[512,2048]{1,0:T(8,128)(2,1)}, u32[]{:S(2)}) %copy-start.1) | copy-done | bytes 2097176
  92.0 25.0 %shard_map.157 = (bf16[128,512]{1,0:T(8,128)(2,1)S(1)}, f32[256,512]{1,0:T(8,128)S(1)}) custom-call(bf16[128,512]{1,0:T(8,128)(2,1)S(1)} %convert_bitcast_fusion.table, bf16[512,512]{1,0:T(8,128)(2,1)S(1)} %bitcast.62, bf16[128,512]{1,0:T(8,128)(2,1)S(1)} %constant_dynamic-slice_fusion.cotangent, bf16[128,512]{1,0:T(8,128)(2,1)S(1)} %copy-done.4, ...), custom_call_target="tpu_custom_call" | custom-call | flops 1000000000 | bytes 10000000 | tf_op jit(solution)/shard_map/pallas_call | solution.py:527
  117.0 2.6 %fusion = bf16[1,2048,512]{2,1,0:T(8,128)(2,1)} fusion(bf16[512,2048]{1,0:T(8,128)(2,1)S(1)} %bitcast.65, bf16[512,512]{1,0:T(8,128)(2,1)S(1)} %copy-done.9), kind=kOutput, calls=%fused_computation.4 | convolution fusion | flops 1074790400 | bytes 4718592 | tf_op jit(solution)/shard_map/dot_general | solution.py:614
  119.7 2.6 %fusion.1 = bf16[1,2048,512]{2,1,0:T(8,128)(2,1)} fusion(bf16[512,2048]{1,0:T(8,128)(2,1)S(1)} %bitcast.66, bf16[512,512]{1,0:T(8,128)(2,1)S(1)} %copy-done.11), kind=kOutput, calls=%fused_computation.5 | convolution fusion | flops 1074790400 | bytes 4718592 | tf_op jit(solution)/shard_map/dot_general | solution.py:617
  122.3 0.7 copy.49
  122.9 0.8 copy.50
  (37 shorter events, 0.5 us)
Async XLA Ops:
  0.6 48.6 %copy-start = (bf16[1,2048,512]{2,1,0:T(8,128)(2,1)S(1)}, bf16[1,2048,512]{2,1,0:T(8,128)(2,1)}, u32[]{:S(2)}) copy-start(bf16[1,2048,512]{2,1,0:T(8,128)(2,1)} %param.21) | copy-start | bytes 6291460
  49.2 1.3 %copy-start.2 = (bf16[8,4,16,2048]{3,2,1,0:T(8,128)(2,1)}, bf16[8,4,16,2048]{3,2,1,0:T(8,128)(2,1)S(1)}, u32[]{:S(2)}) copy-start(bf16[8,4,16,2048]{3,2,1,0:T(8,128)(2,1)S(1)} %get-tuple-element.10) | copy-start | bytes 6291460
  49.2 2.3 %copy-start.7 = (bf16[1,2048,512]{2,1,0:T(8,128)(2,1)S(1)}, bf16[1,2048,512]{2,1,0:T(8,128)(2,1)}, u32[]{:S(2)}) copy-start(bf16[1,2048,512]{2,1,0:T(8,128)(2,1)} %param.22) | copy-start | bytes 6291460
  52.8 2.7 %copy-start.13 = (bf16[1,512,2048]{2,1,0:T(8,128)(2,1)S(1)}, bf16[1,512,2048]{2,1,0:T(8,128)(2,1)}, u32[]{:S(2)}) copy-start(bf16[1,512,2048]{2,1,0:T(8,128)(2,1)} %param.23) | copy-start | bytes 6291460
  57.1 1.3 %copy-start.8 = (bf16[512,512]{1,0:T(8,128)(2,1)}, bf16[512,512]{1,0:T(8,128)(2,1)S(1)}, u32[]{:S(2)}) copy-start(bf16[512,512]{1,0:T(8,128)(2,1)S(1)} %get-tuple-element.14) | copy-start | bytes 1572868
  57.1 1.3 %copy-start.10 = (bf16[512,512]{1,0:T(8,128)(2,1)}, bf16[512,512]{1,0:T(8,128)(2,1)S(1)}, u32[]{:S(2)}) copy-start(bf16[512,512]{1,0:T(8,128)(2,1)S(1)} %get-tuple-element.13) | copy-start | bytes 1572868
  59.9 30.4 %copy-start.12 = (f32[128]{0:T(128)S(1)}, f32[128]{0:T(128)}, u32[]{:S(2)}) copy-start(f32[128]{0:T(128)} %param.17) | copy-start | bytes 1540
  59.9 30.5 %copy-start.4 = (bf16[128,512]{1,0:T(8,128)(2,1)S(1)}, bf16[128,512]{1,0:T(8,128)(2,1)}, u32[]{:S(2)}) copy-start(bf16[128,512]{1,0:T(8,128)(2,1)} %saved.1) | copy-start | bytes 393220
  59.9 30.5 %copy-start.5 = (f32[31,512]{1,0:T(8,128)S(1)}, f32[31,512]{1,0:T(8,128)}, u32[]{:S(2)}) copy-start(f32[31,512]{1,0:T(8,128)} %taps.1) | copy-start | bytes 190468
  59.9 30.5 %copy-start.6 = (f32[512]{0:T(512)S(1)}, f32[512]{0:T(512)}, u32[]{:S(2)}) copy-start(f32[512]{0:T(512)} %param.18) | copy-start | bytes 6148
  90.4 1.6 %copy-start.1 = (bf16[512,2048]{1,0:T(8,128)(2,1)S(1)}, bf16[512,2048]{1,0:T(8,128)(2,1)}, u32[]{:S(2)}) copy-start(bf16[512,2048]{1,0:T(8,128)(2,1)} %weight.1) | copy-start | bytes 6291460
  92.0 25.0 %copy-start.3 = (bf16[8,4,16,2048]{3,2,1,0:T(8,128)(2,1)S(1)}, bf16[8,4,16,2048]{3,2,1,0:T(8,128)(2,1)}, u32[]{:S(2)}) copy-start(bf16[8,4,16,2048]{3,2,1,0:T(8,128)(2,1)} %copy-done.2) | copy-start | bytes 6291460
  92.0 25.0 %copy-start.9 = (bf16[512,512]{1,0:T(8,128)(2,1)S(1)}, bf16[512,512]{1,0:T(8,128)(2,1)}, u32[]{:S(2)}) copy-start(bf16[512,512]{1,0:T(8,128)(2,1)} %copy-done.8) | copy-start | bytes 1572868
  117.0 2.6 %copy-start.11 = (bf16[512,512]{1,0:T(8,128)(2,1)S(1)}, bf16[512,512]{1,0:T(8,128)(2,1)}, u32[]{:S(2)}) copy-start(bf16[512,512]{1,0:T(8,128)(2,1)} %copy-done.10) | copy-start | bytes 1572868

commit v2 on v1

--- a/solution.py
+++ b/solution.py
@@ -6,25 +6,6 @@
 from jax.experimental import pallas as pl
 from jax.experimental.pallas import tpu as pltpu
 from jax.sharding import PartitionSpec as P
-
-
-def route_table(expert_ids, route_weight, slot_start, slot_span, capacity, experts):
-    onehot = (expert_ids[:, :, None] == jnp.arange(experts, dtype=jnp.int32)[None, None, :]).astype(
-        jnp.int32
-    )
-    flat_hot = onehot.reshape(-1, experts)
-    ranks = jnp.cumsum(flat_hot, axis=0) - flat_hot
-    rank_pair = jnp.sum(ranks * flat_hot, axis=1).reshape(expert_ids.shape)
-    slot_index = expert_ids * capacity + rank_pair
-    targets = (
-        jnp.arange(experts, dtype=jnp.int32)[:, None] * capacity
-        + slot_start
-        + jnp.arange(slot_span, dtype=jnp.int32)[None, :]
-    ).reshape(-1)
-    matched = slot_index[None, :, :] == targets[:, None, None]
-    dispatch = jnp.any(matched, axis=2).astype(jnp.bfloat16)
-    slot_weight = jnp.sum(jnp.where(matched, route_weight[None, :, :], 0.0), axis=(1, 2))
-    return (dispatch, slot_weight)
 
 
 def remote(source, target, send_sem, recv_sem, device):
@@ -38,19 +19,40 @@
     )
 
 
-def dispatch_kernel(experts, groups, *refs):
-    sent = refs[:2]
-    held = refs[2:4]
-    local_sem, far_send, far_recv, row_send, row_recv, pair_send, pair_recv = refs[4:]
+CONTRACT_LAST = (((1,), (1,)), ((), ()))
+CONTRACT_FIRST = (((0,), (0,)), ((), ()))
+
+
+def expert_kernel(
+    experts, groups, ids, route, mixer, cotangent, gate_far, up_far, down_far,
+    home, grad_gate, grad_up, grad_down, table,
+    rows, grads, sent_rows, sent_grads, gate, up, down, hidden_gate, hidden_up, active,
+    grad_hg, grad_hu, partial, pair_in, row_out, row_in, total, slot_weight, *sems
+):
+    (load_sem, far_send, far_recv, row_send, row_recv, pair_send, pair_recv,
+     home_send, home_recv, sum_send, sum_recv, back_send, back_recv) = sems
     mine = lax.axis_index("sp")
     place = lax.axis_index("tp")
     chips = groups // 2
     chip, core = place // 2, place % 2
     sibling = chip * 2 + 1 - core
+    tok = mixer.shape[0]
+    capacity, share = rows.shape[2:]
+    slots = experts * capacity
+    ff = gate.shape[1]
+    middle = experts // 2
+    sent = (sent_rows, sent_grads)
+    held = (rows, grads)
 
     def at_chip(step):
         return ((chip + step) % chips) * 2 + core
 
+    loads = [
+        pltpu.make_async_copy(source, target, load_sem.at[at])
+        for at, (source, target) in enumerate(((gate_far, gate), (up_far, up), (down_far, down)))
+    ]
+    for load in loads:
+        load.start()
     barrier = pltpu.get_barrier_semaphore()
 
     def greet(step, carry):
@@ -64,31 +66,54 @@
                             device_id_type=pl.DeviceIdType.MESH)
     pl.semaphore_signal(barrier, inc=1, device_id=(mine, sibling),
                         device_id_type=pl.DeviceIdType.MESH)
+
+    expert = lax.broadcasted_iota(jnp.int32, (experts, tok), 0)
+    hot = [(ids[k : k + 1] == expert).astype(jnp.float32) for k in range(ids.shape[0])]
+    before = lax.broadcasted_iota(jnp.int32, (tok, tok), 0)
+    after = lax.broadcasted_iota(jnp.int32, (tok, tok), 1)
+    rank = jnp.dot(
+        sum(hot).astype(jnp.bfloat16),
+        (before < after).astype(jnp.float32).astype(jnp.bfloat16),
+        preferred_element_type=jnp.float32,
+    )
+    slot = expert.astype(jnp.float32) * capacity + rank
+    number = lax.broadcasted_iota(jnp.int32, (slots, tok), 0).astype(jnp.float32)
+    chosen = jnp.zeros((slots, tok), jnp.float32)
+    weighted = jnp.zeros((slots, tok), jnp.float32)
+    for k in range(ids.shape[0]):
+        match = number == jnp.sum(hot[k] * slot, axis=0, keepdims=True)
+        chosen = jnp.where(match, 1.0, chosen)
+        weighted = jnp.where(match, route[k : k + 1], weighted)
+    table[...] = chosen.astype(jnp.bfloat16).reshape(experts, capacity, tok)
+    slot_weight[...] = jnp.sum(weighted, axis=1, keepdims=True).reshape(experts, capacity, 1)
+    columns = pl.ds(pl.multiple_of(place * share, share), share)
+    every = table[...].reshape(slots, tok)
+    scale = slot_weight[...].reshape(slots, 1)
+    sent_rows[...] = (
+        jnp.dot(every, mixer[:, columns], preferred_element_type=jnp.float32)
+        .astype(jnp.bfloat16).reshape(experts, capacity, share)
+    )
+    sent_grads[...] = (
+        (scale * jnp.dot(every, cotangent[:, columns], preferred_element_type=jnp.float32))
+        .astype(jnp.bfloat16).reshape(experts, capacity, share)
+    )
     pl.semaphore_wait(barrier, experts - 1 + chips)
 
     def far(a, step):
         peer = (mine + step) % experts
-        return remote(sent[a].at[peer], held[a].at[mine, place],
+        return remote(sent[a].at[peer], held[a].at[step, place],
                       far_send.at[a, step], far_recv.at[a, step], (peer, place))
 
     def row(a, step, hop):
-        source = (mine + experts - step) % experts
-        block = held[a].at[source, place]
+        block = held[a].at[step, place]
         return remote(block, block, row_send.at[a, step, hop], row_recv.at[a, step, hop],
                       (mine, at_chip(hop)))
 
     def pair(a, step, hop):
-        source = (mine + experts - step) % experts
-        block = held[a].at[source, at_chip(chips - hop)]
+        block = held[a].at[step, at_chip(chips - hop)]
         return remote(block, block, pair_send.at[a, step, hop], pair_recv.at[a, step, hop],
                       (mine, sibling))
 
-    own = [
-        pltpu.make_async_copy(sent[a].at[mine], held[a].at[mine, place], local_sem.at[a])
-        for a in range(2)
-    ]
-    for a in range(2):
-        own[a].start()
     for a in range(2):
         def start_far(step, carry, a=a):
             far(a, step).start()
@@ -96,185 +121,237 @@
 
         lax.fori_loop(1, experts, start_far, 0)
 
-    def pass_on(a, step):
+    own = table[mine]
+    own_scale = slot_weight[mine]
+    for g in range(groups):
+        span = slice(g * share, (g + 1) * share)
+        rows[0, g] = jnp.dot(
+            own, mixer[:, span], preferred_element_type=jnp.float32
+        ).astype(jnp.bfloat16)
+        grads[0, g] = (
+            own_scale * jnp.dot(own, cotangent[:, span], preferred_element_type=jnp.float32)
+        ).astype(jnp.bfloat16)
+
+    def each(low, high, act):
+        def body(step, carry):
+            act(step)
+            return carry
+
+        lax.fori_loop(low, high, body, 0)
+
+    def service(a, step):
+        far(a, step).wait_recv()
         for hop in range(1, chips):
             row(a, step, hop).start()
         pair(a, step, 0).start()
 
-    def pass_rows(a, step):
+    def settle(a, step):
         for hop in range(1, chips):
             row(a, step, hop).wait_recv()
             pair(a, step, hop).start()
 
-    for a in range(2):
-        own[a].wait()
-        pass_on(a, 0)
-    for a in range(2):
-        def arrive(step, carry, a=a):
-            far(a, step).wait_recv()
-            pass_on(a, step)
-            pass_rows(a, step - 1)
-            return carry
-
-        lax.fori_loop(1, experts, arrive, 0)
-        pass_rows(a, experts - 1)
-    for a in range(2):
-        def finish(step, carry, a=a):
+    def complete(a, step):
+        for hop in range(chips):
+            pair(a, step, hop).wait_recv()
+
+    def both(a):
+        def act(step):
+            service(a, step)
+            settle(a, step - 2)
+        return act
+
+    def chunk(ref, at, g):
+        return ref[at * middle : (at + 1) * middle, g].reshape(middle * capacity, share)
+
+    def lines(at):
+        return slice(at * middle * capacity, (at + 1) * middle * capacity)
+
+    def ahead(at):
+        for weight, result in ((gate, hidden_gate), (up, hidden_up)):
+            value = None
+            for g in range(groups):
+                term = jnp.dot(
+                    chunk(rows, at, g), weight[g * share : (g + 1) * share, :],
+                    preferred_element_type=jnp.float32,
+                )
+                value = term if value is None else value + term
+            result[lines(at), :] = value
+
+    def back(at):
+        value = None
+        for g in range(groups):
+            term = lax.dot_general(
+                chunk(grads, at, g), down[:, g * share : (g + 1) * share], CONTRACT_LAST,
+                preferred_element_type=jnp.float32,
+            )
+            value = term if value is None else value + term
+        hg = hidden_gate[lines(at), :]
+        hu = hidden_up[lines(at), :]
+        sigma = sigmoid(hg)
+        swish = hg * sigma
+        active[lines(at), :] = (swish * hu).astype(jnp.bfloat16)
+        grad_hg[lines(at), :] = (value * hu * sigma * (1.0 + hg * (1.0 - sigma))).astype(jnp.bfloat16)
+        grad_hu[lines(at), :] = (value * swish).astype(jnp.bfloat16)
+        for g in range(groups):
+            term = lax.dot_general(
+                grad_hg[lines(at), :], gate[g * share : (g + 1) * share, :], CONTRACT_LAST,
+                preferred_element_type=jnp.float32,
+            ) + lax.dot_general(
+                grad_hu[lines(at), :], up[g * share : (g + 1) * share, :], CONTRACT_LAST,
+                preferred_element_type=jnp.float32,
+            )
+            partial[g, at * middle : (at + 1) * middle] = term.astype(jnp.bfloat16).reshape(
+                middle, capacity, share
+            )
+
+    def weight_grads(g):
+        span = pl.ds(pl.multiple_of(g * share, share), share)
+        left = rows[:, g].reshape(slots, share)
+        grad_gate[span, :] = lax.dot_general(
+            left, grad_hg[...], CONTRACT_FIRST, preferred_element_type=jnp.float32
+        ).astype(jnp.bfloat16)
+        grad_up[span, :] = lax.dot_general(
+            left, grad_hu[...], CONTRACT_FIRST, preferred_element_type=jnp.float32
+        ).astype(jnp.bfloat16)
+        grad_down[:, span] = lax.dot_general(
+            active[...], grads[:, g].reshape(slots, share), CONTRACT_FIRST,
+            preferred_element_type=jnp.float32,
+        ).astype(jnp.bfloat16)
+
+    def home_pair(step, hop):
+        other = ((chip + hop) % chips) * 2 + 1 - core
+        return remote(partial.at[other, step], pair_in.at[hop, step],
+                      home_send.at[step, hop], home_recv.at[step, hop], (mine, sibling))
+
+    def home_row(step, hop):
+        return remote(row_out.at[hop, step], row_in.at[hop, step],
+                      sum_send.at[step, hop], sum_recv.at[step, hop], (mine, at_chip(hop)))
+
+    def home_far(step):
+        owner = (mine + experts - step) % experts
+        return remote(total.at[step], home.at[mine],
+                      back_send.at[step], back_recv.at[step], (owner, place))
+
+    def start_pair(step):
+        for hop in reversed(range(chips)):
+            home_pair(step, hop).start()
+
+    def add_pair(step, hop):
+        home_pair(step, hop).wait_recv()
+        return partial[at_chip(hop), step].astype(jnp.float32) + pair_in[hop, step].astype(
+            jnp.float32
+        )
+
+    def send_rows(step):
+        for hop in range(1, chips):
+            row_out[hop, step] = add_pair(step, hop).astype(row_out.dtype)
+            home_row(step, hop).start()
+
+    def add_rows(step):
+        value = add_pair(step, 0)
+        for hop in range(1, chips):
+            home_row(step, hop).wait_recv()
+            value = value + row_in[hop, step].astype(jnp.float32)
+        return value.astype(total.dtype)
+
+    def send_home(step):
+        total[step] = add_rows(step)
+        home_far(step).start()
+
+    each(1, 3, functools.partial(service, 0))
+    each(3, experts, both(0))
+    service(1, 1)
+    settle(0, experts - 2)
+    service(1, 2)
+    settle(0, experts - 1)
+    loads[0].wait()
+    loads[1].wait()
+    each(1, middle, functools.partial(complete, 0))
+    ahead(0)
+    each(3, middle + 1, both(1))
+    each(middle, experts, functools.partial(complete, 0))
+    ahead(1)
+    each(middle + 1, middle + 2, both(1))
+    loads[2].wait()
+    each(1, middle, functools.partial(complete, 1))
+    back(0)
+    each(0, middle, start_pair)
+    each(middle + 2, experts, both(1))
+    settle(1, experts - 2)
+    settle(1, experts - 1)
+    each(0, middle, send_rows)
+    each(middle, experts, functools.partial(complete, 1))
+    back(1)
+    each(middle, experts, start_pair)
+    weight_grads(0)
+    home[mine] = add_rows(0)
+    each(1, middle, send_home)
+    each(middle, experts, send_rows)
+    each(1, groups - 1, weight_grads)
+    each(middle, experts, send_home)
+    weight_grads(groups - 1)
+
+    def finish(step):
+        for hop in range(chips):
+            home_pair(step, hop).wait_send()
+            if hop:
+                home_row(step, hop).wait_send()
+
+    def finish_far(step):
+        home_far(step).wait()
+        for a in range(2):
+            far(a, step).wait_send()
             for hop in range(chips):
-                pair(a, step, hop).wait()
+                pair(a, step, hop).wait_send()
                 if hop:
                     row(a, step, hop).wait_send()
-            return carry
-
-        lax.fori_loop(0, experts, finish, 0)
-
-        def finish_far(step, carry, a=a):
-            far(a, step).wait_send()
-            return carry
-
-        lax.fori_loop(1, experts, finish_far, 0)
-
-
-def dispatch_blocks(rows, grads, groups):
-    experts, span, width = rows.shape
+
+    each(0, experts, finish)
+    each(1, experts, finish_far)
+
+
+def expert_blocks(ids, route, mixer, cotangent, gate, up, down, experts, groups):
+    tok, width = mixer.shape
+    ff = gate.shape[1]
+    share = width // groups
+    capacity = groups * max(1, 4 * tok // (experts * groups))
     chips = groups // 2
-    full = jax.ShapeDtypeStruct((experts, groups, span, width), rows.dtype)
+    slots = experts * capacity
+    half = jnp.bfloat16
     dma = pltpu.SemaphoreType.DMA
+    vmem = pl.BlockSpec(memory_space=pltpu.VMEM)
+    held = pltpu.VMEM((experts, groups, capacity, share), half)
+    sent = pltpu.VMEM((experts, capacity, share), half)
+    blocks = pltpu.VMEM((chips, experts, capacity, share), half)
     return pl.pallas_call(
-        functools.partial(dispatch_kernel, experts, groups),
-        out_shape=(full, full),
-        in_specs=[pl.BlockSpec(memory_space=pltpu.VMEM)] * 2,
-        out_specs=[pl.BlockSpec(memory_space=pltpu.VMEM)] * 2,
-        scratch_shapes=[dma((2,))]
+        functools.partial(expert_kernel, experts, groups),
+        out_shape=(
+            jax.ShapeDtypeStruct((experts, capacity, share), half),
+            jax.ShapeDtypeStruct(gate.shape, half),
+            jax.ShapeDtypeStruct(up.shape, half),
+            jax.ShapeDtypeStruct(down.shape, half),
+            jax.ShapeDtypeStruct((experts, capacity, tok), half),
+        ),
+        in_specs=[vmem] * 4 + [pl.BlockSpec(memory_space=pl.ANY)] * 3,
+        out_specs=[vmem] * 5,
+        scratch_shapes=[held] * 2
+        + [sent] * 2
+        + [pltpu.VMEM(array.shape, half) for array in (gate, up, down)]
+        + [pltpu.VMEM((slots, ff), jnp.float32)] * 2
+        + [pltpu.VMEM((slots, ff), half)] * 3
+        + [pltpu.VMEM((groups, experts, capacity, share), half)]
+        + [blocks] * 3
+        + [sent, pltpu.VMEM((experts, capacity, 1), jnp.float32)]
+        + [dma((3,))]
         + [dma((2, experts))] * 2
-        + [dma((2, experts, chips))] * 4,
-        compiler_params=pltpu.CompilerParams(
-            collective_id=0, has_side_effects=True, vmem_limit_bytes=24 * 2**20
-        ),
-        cost_estimate=pl.CostEstimate(
-            flops=0, bytes_accessed=40 * full.size, transcendentals=0
-        ),
-    )(rows, grads)
-
-
-def home_kernel(experts, groups, partial, home, pair_in, row_out, row_in, total, *sems):
-    pair_send, pair_recv, row_send, row_recv, far_send, far_recv = sems
-    mine = lax.axis_index("sp")
-    place = lax.axis_index("tp")
-    chips = groups // 2
-    chip, core = place // 2, place % 2
-    sibling = chip * 2 + 1 - core
-
-    def at_chip(step):
-        return ((chip + step) % chips) * 2 + core
-
-    barrier = pltpu.get_barrier_semaphore()
-
-    def greet(step, carry):
-        pl.semaphore_signal(barrier, inc=1, device_id=((mine + step) % experts, place),
-                            device_id_type=pl.DeviceIdType.MESH)
-        return carry
-
-    lax.fori_loop(1, experts, greet, 0)
-    for step in range(1, chips):
-        pl.semaphore_signal(barrier, inc=1, device_id=(mine, at_chip(step)),
-                            device_id_type=pl.DeviceIdType.MESH)
-    pl.semaphore_signal(barrier, inc=1, device_id=(mine, sibling),
-                        device_id_type=pl.DeviceIdType.MESH)
-    pl.semaphore_wait(barrier, experts - 1 + chips)
-
-    def pair(step, hop):
-        owner = (mine + step + 1) % experts
-        other = ((chip + hop) % chips) * 2 + 1 - core
-        return remote(partial.at[other, owner], pair_in.at[hop, owner],
-                      pair_send.at[step, hop], pair_recv.at[step, hop], (mine, sibling))
-
-    def row(step, hop):
-        owner = (mine + step + 1) % experts
-        return remote(row_out.at[hop, owner], row_in.at[hop, owner],
-                      row_send.at[step, hop], row_recv.at[step, hop], (mine, at_chip(hop)))
-
-    def far(step):
-        owner = (mine + step + 1) % experts
-        return remote(total.at[owner], home.at[mine],
-                      far_send.at[step], far_recv.at[step], (owner, place))
-
-    def start_pair(step, carry):
-        for hop in reversed(range(chips)):
-            pair(step, hop).start()
-        return carry
-
-    lax.fori_loop(0, experts, start_pair, 0)
-
-    def add_pair(step, hop):
-        owner = (mine + step + 1) % experts
-        pair(step, hop).wait_recv()
-        return partial[at_chip(hop), owner].astype(jnp.float32) + pair_in[hop, owner].astype(
-            jnp.float32
-        )
-
-    def send_rows(step):
-        owner = (mine + step + 1) % experts
-        for hop in range(1, chips):
-            row_out[hop, owner] = add_pair(step, hop).astype(row_out.dtype)
-            row(step, hop).start()
-
-    def add_rows(step):
-        owner = (mine + step + 1) % experts
-        value = add_pair(step, 0)
-        for hop in range(1, chips):
-            row(step, hop).wait_recv()
-            value = value + row_in[hop, owner].astype(jnp.float32)
-        return value.astype(total.dtype)
-
-    def advance(step, carry):
-        send_rows(step)
-        before = step - 1
-        total[(mine + before + 1) % experts] = add_rows(before)
-        far(before).start()
-        return carry
-
-    send_rows(0)
-    lax.fori_loop(1, experts, advance, 0)
-    home[mine] = add_rows(experts - 1)
-
-    def finish(step, carry):
-        for hop in range(chips):
-            pair(step, hop).wait_send()
-            if hop:
-                row(step, hop).wait_send()
-        return carry
-
-    lax.fori_loop(0, experts, finish, 0)
-
-    def finish_far(step, carry):
-        far(step).wait()
-        return carry
-
-    lax.fori_loop(0, experts - 1, finish_far, 0)
-
-
-def home_blocks(partial):
-    groups, experts, capacity, share = partial.shape
-    chips = groups // 2
-    dma = pltpu.SemaphoreType.DMA
-    blocks = pltpu.VMEM((chips, experts, capacity, share), partial.dtype)
-    return pl.pallas_call(
-        functools.partial(home_kernel, experts, groups),
-        out_shape=jax.ShapeDtypeStruct((experts, capacity, share), partial.dtype),
-        in_specs=[pl.BlockSpec(memory_space=pltpu.VMEM)],
-        out_specs=pl.BlockSpec(memory_space=pltpu.VMEM),
-        scratch_shapes=[blocks] * 3
-        + [pltpu.VMEM((experts, capacity, share), partial.dtype)]
+        + [dma((2, experts, chips))] * 4
         + [dma((experts, chips))] * 4
         + [dma((experts,))] * 2,
         compiler_params=pltpu.CompilerParams(
-            collective_id=1, has_side_effects=True, vmem_limit_bytes=24 * 2**20
+            collective_id=0, has_side_effects=True, vmem_limit_bytes=48 * 2**20
         ),
-        cost_estimate=pl.CostEstimate(
-            flops=0, bytes_accessed=40 * partial.size, transcendentals=0
-        ),
-    )(partial)
+        cost_estimate=pl.CostEstimate(flops=10**10, bytes_accessed=10**7, transcendentals=0),
+    )(ids, route, mixer, cotangent, gate, up, down)
 
 
 def line_width(experts):
@@ -356,7 +433,9 @@
         return remote(share_at(owner), share_at(owner), pair_send.at[hop], pair_recv.at[hop],
                       (mine, sibling))
 
-    share = jnp.dot(table[...], home[...], preferred_element_type=jnp.float32)
+    share = lax.dot_general(
+        table[...], home[...], CONTRACT_FIRST, preferred_element_type=jnp.float32
+    )
     share = (share + cotangent[...].astype(jnp.float32)).astype(jnp.bfloat16)
     for part in range(per):
         piece = share[:, part * width : (part + 1) * width]
@@ -570,66 +649,23 @@
 ):
     experts = lax.axis_size("sp")
     groups = lax.axis_size("tp")
-    tok_rows, model_width = cotangent.shape
-    capacity = groups * max(1, 4 * tok_rows // (experts * groups))
-    slot_span = capacity // groups
-    slot_start = lax.axis_index("tp") * slot_span
-    dispatch, slot_weight = route_table(
-        expert_ids, route_weight, slot_start, slot_span, capacity, experts
-    )
-    sent_rows = jnp.dot(dispatch, mixer_out, preferred_element_type=jnp.float32).astype(
-        jnp.bfloat16
-    )
-    sent_grad = (
-        slot_weight[:, None] * jnp.dot(dispatch, cotangent, preferred_element_type=jnp.float32)
-    ).astype(jnp.bfloat16)
-    sent_rows = sent_rows.reshape(experts, slot_span, model_width)
-    sent_grad = sent_grad.reshape(experts, slot_span, model_width)
-    routed_rows, routed_grad = dispatch_blocks(sent_rows, sent_grad, groups)
-    full_table, unused_weight = route_table(
-        expert_ids, route_weight, 0, capacity, capacity, experts
-    )
-    routed_rows = routed_rows.reshape(-1, model_width)
-    routed_grad = routed_grad.reshape(-1, model_width)
-    w_first = gate_weight[0]
-    w_third = up_weight[0]
-    w_second = down_weight[0]
-    contract_last = (((1,), (1,)), ((), ()))
-    contract_first = (((0,), (0,)), ((), ()))
-    hidden_gate = jnp.dot(routed_rows, w_first, preferred_element_type=jnp.float32)
-    hidden_up = jnp.dot(routed_rows, w_third, preferred_element_type=jnp.float32)
-    sigma = jax.nn.sigmoid(hidden_gate)
-    swish = hidden_gate * sigma
-    activ = (swish * hidden_up).astype(jnp.bfloat16)
-    grad_second = lax.dot_general(
-        activ, routed_grad, contract_first, preferred_element_type=jnp.float32
-    ).astype(jnp.bfloat16)
-    grad_activ = lax.dot_general(
-        routed_grad, w_second, contract_last, preferred_element_type=jnp.float32
-    )
-    grad_gpre = (grad_activ * hidden_up * sigma * (1.0 + hidden_gate * (1.0 - sigma))).astype(
-        jnp.bfloat16
-    )
-    grad_upre = (grad_activ * swish).astype(jnp.bfloat16)
-    grad_first = lax.dot_general(
-        routed_rows, grad_gpre, contract_first, preferred_element_type=jnp.float32
-    ).astype(jnp.bfloat16)
-    grad_third = lax.dot_general(
-        routed_rows, grad_upre, contract_first, preferred_element_type=jnp.float32
-    ).astype(jnp.bfloat16)
-    partial_value = lax.dot_general(
-        grad_gpre, w_first, contract_last, preferred_element_type=jnp.float32
-    ) + lax.dot_general(grad_upre, w_third, contract_last, preferred_element_type=jnp.float32)
-    share = model_width // groups
-    partial_groups = jnp.transpose(
-        partial_value.astype(jnp.bfloat16).reshape(-1, groups, share), (1, 0, 2)
-    )
-    home_rows = home_blocks(partial_groups.reshape(groups, experts, capacity, share))
+    share = cotangent.shape[1] // groups
+    home_rows, grad_first, grad_third, grad_second, table = expert_blocks(
+        jnp.transpose(expert_ids),
+        jnp.transpose(route_weight),
+        mixer_out,
+        cotangent,
+        gate_weight[0],
+        up_weight[0],
+        down_weight[0],
+        experts,
+        groups,
+    )
     own_cotangent = lax.dynamic_slice_in_dim(
         cotangent, lax.axis_index("tp") * share, share, axis=1
     )
     result, grad_proj = tail_blocks(
-        jnp.transpose(full_table),
+        table.reshape(-1, table.shape[-1]),
         home_rows.reshape(-1, share),
         own_cotangent,
         saved_normalized,

time: 124 us -> 103 us (0.83)
  matrix products: 17.2 us -> 0 us
  Pallas kernels: 95.5 us -> 90.2 us
  local copies, waits for them, and re-layouts: 7.37 us -> 11.6 us
  other arithmetic: 2.67 us -> 0 us
    dot_general x10 -> x0, matrix products: 17.2 us -> none  [the longest x1 2.68 us: shards(): lax.dot_general(activ, routed_grad, contract_first, preferred_element_typ...]
    unnamed x31 -> x23, local copies, waits for them, and re-layouts: 5.13 us -> 9.88 us
    pallas_call x2 -> x1, Pallas kernels: 70.6 us -> 67.4 us  [expert_blocks(): pl.pallas_call(functools.partial(expert_kernel, experts, groups), out_sha...]
    pallas_call x1, Pallas kernels: 25 us -> 22.8 us  [tail_blocks(): pl.pallas_call(functools.partial(tail_kernel, experts, groups, lead), out...]
where the time goes in v2:
time: 103 us; the launch traced here: 102 us
  Pallas kernels  90.2 us (88%)
  local copies, waits for them, and re-layouts  11.6 us (11%)
    pallas_call x1, Pallas kernels, expert_blocks(): pl.pallas_call(functools.partial(expert_kernel, experts, groups), out_sha...  67.4 us
    pallas_call x1, Pallas kernels, tail_blocks(): pl.pallas_call(functools.partial(tail_kernel, experts, groups, lead), out...  22.8 us
    unnamed x23, local copies, waits for them, and re-layouts  9.88 us

profile of v2, /device:TPU:0, one launch (start us, length us, event | category | flops | bytes accessed | tf_op | source)
XLA Modules:
  0.0 102.5 jit_solution(7907495655549446657)
XLA Ops:
  0.6 0.8 copy.17.inverse
  1.4 0.9 constant_dynamic-slice_fusion.cotangent
  2.3 0.0 copy-start
  2.3 1.0 %copy-done = bf16[128,2048]{1,0:T(8,128)(2,1)S(1)} copy-done((bf16[128,2048]{1,0:T(8,128)(2,1)S(1)}, bf16[128,2048]{1,0:T(8,128)(2,1)}, u32[]{:S(2)}) %copy-start) | copy-done | bytes 524312
  3.4 0.0 copy-start.2
  3.4 1.0 %copy-done.2 = bf16[128,2048]{1,0:T(8,128)(2,1)S(1)} copy-done((bf16[128,2048]{1,0:T(8,128)(2,1)S(1)}, bf16[128,2048]{1,0:T(8,128)(2,1)}, u32[]{:S(2)}) %copy-start.2) | copy-done | bytes 524312
  4.4 0.0 copy-start.6
  4.4 0.7 copy-done.6
  5.1 0.0 copy-start.7
  5.1 0.7 copy-done.7
  5.8 0.0 copy-start.1
  5.8 0.0 copy-start.3
  5.8 0.0 copy-start.4
  5.8 0.0 copy-start.5
  5.8 67.4 %shard_map.155 = (bf16[8,64,512]{2,1,0:T(8,128)(2,1)S(1)}, bf16[2048,512]{1,0:T(8,128)(2,1)S(1)}, bf16[2048,512]{1,0:T(8,128)(2,1)S(1)}, bf16[512,2048]{1,0:T(8,128)(2,1)}, bf16[8,64,128]{2,1,0:T(8,128)(2,1)S(1)}) custom-call(s32[2,128]{1,0:T(2,128)S(1)} %bitcast.15, f32[2,128]{1,0:T(2,128)S(1)} %bitcast.16, bf16[128,2048]{1,0:T(8,128)(2,1)S(1)} %copy-done.2, ...), custom_call_target="tpu_custom_call" | custom-call | flops 10000000000 | bytes 10000000 | tf_op jit(solution)/shard_map/pallas_call | solution.py:326
  73.1 0.0 copy-done.1
  73.2 0.0 copy-done.3
  73.2 0.0 copy-done.4
  73.2 0.0 copy-done.5
  73.2 22.8 %shard_map.156 = (bf16[128,512]{1,0:T(8,128)(2,1)S(1)}, f32[256,512]{1,0:T(8,128)S(1)}) custom-call(bf16[512,128]{1,0:T(8,128)(2,1)S(1)} %bitcast.18, bf16[512,512]{1,0:T(8,128)(2,1)S(1)} %bitcast.17, bf16[128,512]{1,0:T(8,128)(2,1)S(1)} %constant_dynamic-slice_fusion.cotangent, bf16[128,512]{1,0:T(8,128)(2,1)S(1)} %copy-done.3, f32[128,1]{1,0:T(8,128)S(1)} %copy.17.inverse, ...), custom_call_target="tpu_custom_call" | custom-call | flops 1000000000 | bytes 10000000 | tf_op jit(solution)/shard_map/pallas_call | solution.py:606
  96.0 0.7 copy.23
  96.7 0.8 copy.24
  97.5 1.3 %copy.25 = bf16[1,2048,512]{2,1,0:T(8,128)(2,1)} copy(bf16[1,2048,512]{2,1,0:T(8,128)(2,1)S(1)} %bitcast.13) | data formatting | bytes 4194304
  98.8 0.0 copy-start.8
  98.8 1.3 %copy.26 = bf16[1,2048,512]{2,1,0:T(8,128)(2,1)} copy(bf16[1,2048,512]{2,1,0:T(8,128)(2,1)S(1)} %bitcast.12) | data formatting | bytes 4194304
  100.1 1.0 %copy-done.8 = bf16[512,2048]{1,0:T(8,128)(2,1)S(1)} copy-done((bf16[512,2048]{1,0:T(8,128)(2,1)S(1)}, bf16[512,2048]{1,0:T(8,128)(2,1)}, u32[]{:S(2)}) %copy-start.8) | copy-done | bytes 2097176
  101.2 1.3 %copy.27 = bf16[1,512,2048]{2,1,0:T(8,128)(2,1)} copy(bf16[1,512,2048]{2,1,0:T(8,128)(2,1)S(1)} %bitcast.19) | data formatting | bytes 4194304
Async XLA Ops:
  2.3 1.0 %copy-start = (bf16[128,2048]{1,0:T(8,128)(2,1)S(1)}, bf16[128,2048]{1,0:T(8,128)(2,1)}, u32[]{:S(2)}) copy-start(bf16[128,2048]{1,0:T(8,128)(2,1)} %cotangent.1) | copy-start | bytes 1572868
  3.4 1.0 %copy-start.2 = (bf16[128,2048]{1,0:T(8,128)(2,1)S(1)}, bf16[128,2048]{1,0:T(8,128)(2,1)}, u32[]{:S(2)}) copy-start(bf16[128,2048]{1,0:T(8,128)(2,1)} %mixer.1) | copy-start | bytes 1572868
  4.4 0.7 copy-start.6
  5.1 0.7 copy-start.7
  5.8 67.4 %copy-start.1 = (bf16[512,2048]{1,0:T(8,128)(2,1)S(1)}, bf16[512,2048]{1,0:T(8,128)(2,1)}, u32[]{:S(2)}) copy-start(bf16[512,2048]{1,0:T(8,128)(2,1)} %weight.1) | copy-start | bytes 6291460
  5.8 67.4 %copy-start.3 = (bf16[128,512]{1,0:T(8,128)(2,1)S(1)}, bf16[128,512]{1,0:T(8,128)(2,1)}, u32[]{:S(2)}) copy-start(bf16[128,512]{1,0:T(8,128)(2,1)} %saved.1) | copy-start | bytes 393220
  5.8 67.4 %copy-start.4 = (f32[31,512]{1,0:T(8,128)S(1)}, f32[31,512]{1,0:T(8,128)}, u32[]{:S(2)}) copy-start(f32[31,512]{1,0:T(8,128)} %taps.1) | copy-start | bytes 190468
  5.8 67.4 %copy-start.5 = (f32[512]{0:T(512)S(1)}, f32[512]{0:T(512)}, u32[]{:S(2)}) copy-start(f32[512]{0:T(512)} %param.18) | copy-start | bytes 6148
  98.8 2.3 %copy-start.8 = (bf16[512,2048]{1,0:T(8,128)(2,1)S(1)}, bf16[512,2048]{1,0:T(8,128)(2,1)}, u32[]{:S(2)}) copy-start(bf16[512,2048]{1,0:T(8,128)(2,1)} %get-tuple-element.18) | copy-start | bytes 6291460

commit v3 on v2

--- a/solution.py
+++ b/solution.py
@@ -24,9 +24,9 @@
 
 
 def expert_kernel(
-    experts, groups, ids, route, mixer, cotangent, gate_far, up_far, down_far,
+    experts, groups, ids_far, route_far, mixer_far, cotangent_far, gate_far, up_far, down_far,
     home, grad_gate, grad_up, grad_down, table,
-    rows, grads, sent_rows, sent_grads, gate, up, down, hidden_gate, hidden_up, active,
+    ids, route, mixer, cotangent, rows, grads, sent_rows, sent_grads, gate, up, down, hidden_gate, hidden_up, active,
     grad_hg, grad_hu, partial, pair_in, row_out, row_in, total, slot_weight, *sems
 ):
     (load_sem, far_send, far_recv, row_send, row_recv, pair_send, pair_recv,
@@ -49,7 +49,12 @@
 
     loads = [
         pltpu.make_async_copy(source, target, load_sem.at[at])
-        for at, (source, target) in enumerate(((gate_far, gate), (up_far, up), (down_far, down)))
+        for at, (source, target) in enumerate(
+            (
+                (ids_far, ids), (route_far, route), (mixer_far, mixer), (cotangent_far, cotangent),
+                (gate_far, gate), (up_far, up), (down_far, down),
+            )
+        )
     ]
     for load in loads:
         load.start()
@@ -67,6 +72,8 @@
     pl.semaphore_signal(barrier, inc=1, device_id=(mine, sibling),
                         device_id_type=pl.DeviceIdType.MESH)
 
+    loads[0].wait()
+    loads[1].wait()
     expert = lax.broadcasted_iota(jnp.int32, (experts, tok), 0)
     hot = [(ids[k : k + 1] == expert).astype(jnp.float32) for k in range(ids.shape[0])]
     before = lax.broadcasted_iota(jnp.int32, (tok, tok), 0)
@@ -89,10 +96,12 @@
     columns = pl.ds(pl.multiple_of(place * share, share), share)
     every = table[...].reshape(slots, tok)
     scale = slot_weight[...].reshape(slots, 1)
+    loads[2].wait()
     sent_rows[...] = (
         jnp.dot(every, mixer[:, columns], preferred_element_type=jnp.float32)
         .astype(jnp.bfloat16).reshape(experts, capacity, share)
     )
+    loads[3].wait()
     sent_grads[...] = (
         (scale * jnp.dot(every, cotangent[:, columns], preferred_element_type=jnp.float32))
         .astype(jnp.bfloat16).reshape(experts, capacity, share)
@@ -264,15 +273,15 @@
     settle(0, experts - 2)
     service(1, 2)
     settle(0, experts - 1)
-    loads[0].wait()
-    loads[1].wait()
+    loads[4].wait()
+    loads[5].wait()
     each(1, middle, functools.partial(complete, 0))
     ahead(0)
     each(3, middle + 1, both(1))
     each(middle, experts, functools.partial(complete, 0))
     ahead(1)
     each(middle + 1, middle + 2, both(1))
-    loads[2].wait()
+    loads[6].wait()
     each(1, middle, functools.partial(complete, 1))
     back(0)
     each(0, middle, start_pair)
@@ -332,9 +341,10 @@
             jax.ShapeDtypeStruct(down.shape, half),
             jax.ShapeDtypeStruct((experts, capacity, tok), half),
         ),
-        in_specs=[vmem] * 4 + [pl.BlockSpec(memory_space=pl.ANY)] * 3,
+        in_specs=[pl.BlockSpec(memory_space=pltpu.HBM)] * 7,
         out_specs=[vmem] * 5,
-        scratch_shapes=[held] * 2
+        scratch_shapes=[pltpu.VMEM(array.shape, array.dtype) for array in (ids, route, mixer, cotangent)]
+        + [held] * 2
         + [sent] * 2
         + [pltpu.VMEM(array.shape, half) for array in (gate, up, down)]
         + [pltpu.VMEM((slots, ff), jnp.float32)] * 2
@@ -342,16 +352,21 @@
         + [pltpu.VMEM((groups, experts, capacity, share), half)]
         + [blocks] * 3
         + [sent, pltpu.VMEM((experts, capacity, 1), jnp.float32)]
-        + [dma((3,))]
+        + [dma((7,))]
         + [dma((2, experts))] * 2
         + [dma((2, experts, chips))] * 4
         + [dma((experts, chips))] * 4
         + [dma((experts,))] * 2,
         compiler_params=pltpu.CompilerParams(
-            collective_id=0, has_side_effects=True, vmem_limit_bytes=48 * 2**20
+            collective_id=0, has_side_effects=True, vmem_limit_bytes=36 * 2**20
         ),
         cost_estimate=pl.CostEstimate(flops=10**10, bytes_accessed=10**7, transcendentals=0),
-    )(ids, route, mixer, cotangent, gate, up, down)
+    )(
+        *(
+            pltpu.with_memory_space_constraint(array, pltpu.HBM)
+            for array in (ids, route, mixer, cotangent, gate, up, down)
+        )
+    )
 
 
 def line_width(experts):
@@ -366,8 +381,8 @@
 
 
 def tail_kernel(
-    experts, groups, lead, table, home, cotangent, saved, inverse, gain, taps, weight, result,
-    grad_proj, blocks, every, acts, sums, extended, *sems
+    experts, groups, lead, table, home, cotangent_far, saved, inverse, gain, weight,
+    every, acts, extended, cotangent, blocks, sums, load_sem, *sems
 ):
     (row_send, row_recv, pair_send, pair_recv, far_send, far_recv, half_send, half_recv,
      line_send, line_recv, side_send, side_recv, sum_send, sum_recv, halo_send, halo_recv) = sems
@@ -387,6 +402,12 @@
     def at_chip(step):
         return ((chip + step) % chips) * 2 + core
 
+    part_width = cotangent.shape[1]
+    load = pltpu.make_async_copy(
+        cotangent_far.at[:, pl.ds(pl.multiple_of(place * part_width, part_width), part_width)],
+        cotangent, load_sem,
+    )
+    load.start()
     barrier = pltpu.get_barrier_semaphore()
 
     def greet(step, carry):
@@ -436,6 +457,7 @@
     share = lax.dot_general(
         table[...], home[...], CONTRACT_FIRST, preferred_element_type=jnp.float32
     )
+    load.wait()
     share = (share + cotangent[...].astype(jnp.float32)).astype(jnp.bfloat16)
     for part in range(per):
         piece = share[:, part * width : (part + 1) * width]
@@ -517,8 +539,9 @@
         return jnp.transpose(jnp.broadcast_to(flat, (lanes, tok)))
 
     mean, slope = column(0), column(1)
+    deviation = jnp.transpose(jnp.broadcast_to(inverse[...], (lanes, tok)))
     for at in range(0, channels, lanes):
-        extended[at // lanes, 0:tok] = inverse[...] * (
+        extended[at // lanes, 0:tok] = deviation * (
             grad[:, at : at + lanes] - mean - normalized[:, at : at + lanes] * slope
         )
     reach = extended.shape[1] - tok
@@ -549,12 +572,6 @@
     @pl.when(mine < experts - 1)
     def _():
         halo().wait_recv()
-
-    for at in range(0, channels, lanes):
-        value = jnp.zeros((tok, lanes), jnp.float32)
-        for tap in range(taps.shape[0]):
-            value = value + taps[tap : tap + 1, at : at + lanes] * extended[at // lanes, tap : tap + tok]
-        result[:, at : at + lanes] = value.astype(result.dtype)
 
     def arrive(step, carry):
         to_half(step).wait_recv()
@@ -564,13 +581,6 @@
     for step in range(across):
         for hop in range(1, lead):
             beside(step, hop).wait_recv()
-    grad_proj[...] = lax.dot_general(
-        every[...].reshape(experts * tok, width),
-        acts[...].reshape(experts * tok, channels),
-        (((0,), (0,)), ((), ())),
-        preferred_element_type=jnp.float32,
-    )
-
     @pl.when(mine > 0)
     def _():
         halo().wait_send()
@@ -593,30 +603,29 @@
     lax.fori_loop(1, experts, finish, 0)
 
 
-def tail_blocks(table, home, cotangent, saved, inverse, gain, taps, weight, experts, groups):
+def tail_blocks(table, home, cotangent, saved, inverse, gain, weight, reach, experts, groups):
     tok, channels = saved.shape
     model_width = weight.shape[1]
     width = model_width // experts
     lead = line_width(experts)
     across = experts // lead
     lanes = min(channels, 128)
-    reach = (taps.shape[0] + 6) // 8 * 8
     dma = pltpu.SemaphoreType.DMA
     vmem = pl.BlockSpec(memory_space=pltpu.VMEM)
     return pl.pallas_call(
         functools.partial(tail_kernel, experts, groups, lead),
         out_shape=(
-            jax.ShapeDtypeStruct((tok, channels), jnp.bfloat16),
-            jax.ShapeDtypeStruct((width, channels), jnp.float32),
+            jax.ShapeDtypeStruct((experts, 2, tok // 2, width), jnp.bfloat16),
+            jax.ShapeDtypeStruct((experts, tok, channels), jnp.bfloat16),
+            jax.ShapeDtypeStruct((channels // lanes, tok + reach, lanes), jnp.float32),
         ),
-        in_specs=[vmem] * 8,
-        out_specs=[vmem] * 2,
+        in_specs=[vmem] * 2 + [pl.BlockSpec(memory_space=pltpu.HBM)] + [vmem] * 4,
+        out_specs=[vmem] * 3,
         scratch_shapes=[
+            pltpu.VMEM((tok, model_width // groups), jnp.bfloat16),
             pltpu.VMEM((experts, 2, tok // 2, width), jnp.bfloat16),
-            pltpu.VMEM((experts, 2, tok // 2, width), jnp.bfloat16),
-            pltpu.VMEM((experts, tok, channels), jnp.bfloat16),
             pltpu.VMEM((groups, 2, 8, tok), jnp.float32),
-            pltpu.VMEM((channels // lanes, tok + reach, lanes), jnp.float32),
+            dma,
         ]
         + [dma((groups // 2,))] * 4
         + [dma((experts,))] * 4
@@ -625,12 +634,69 @@
         + [dma((groups,))] * 2
         + [dma] * 2,
         compiler_params=pltpu.CompilerParams(
-            collective_id=2, has_side_effects=True, vmem_limit_bytes=32 * 2**20
+            collective_id=2, has_side_effects=True, vmem_limit_bytes=16 * 2**20
         ),
         cost_estimate=pl.CostEstimate(
             flops=10**9, bytes_accessed=10**7, transcendentals=0
         ),
-    )(table, home, cotangent, saved, inverse, gain, taps, weight)
+    )(
+        table, home, pltpu.with_memory_space_constraint(cotangent, pltpu.HBM), saved, inverse,
+        gain, weight,
+    )
+
+
+def last_kernel(
+    every, acts, extended, taps, gate, up, down, result_far, proj_far, gate_far, up_far, down_far,
+    result, proj, sems
+):
+    stores = [
+        pltpu.make_async_copy(source, target, sems.at[at])
+        for at, (source, target) in enumerate(
+            (
+                (gate, gate_far), (up, up_far), (down, down_far), (result, result_far),
+                (proj, proj_far),
+            )
+        )
+    ]
+    for store in stores[:3]:
+        store.start()
+    tok, channels = result.shape
+    lanes = extended.shape[-1]
+    for at in range(0, channels, lanes):
+        value = jnp.zeros((tok, lanes), jnp.float32)
+        for tap in range(taps.shape[0]):
+            value = value + taps[tap : tap + 1, at : at + lanes] * extended[at // lanes, tap : tap + tok]
+        result[:, at : at + lanes] = value.astype(result.dtype)
+    stores[3].start()
+    proj[...] = lax.dot_general(
+        every[...].reshape(-1, every.shape[-1]),
+        acts[...].reshape(-1, channels),
+        CONTRACT_FIRST,
+        preferred_element_type=jnp.float32,
+    )
+    stores[4].start()
+    for store in stores:
+        store.wait()
+
+
+def last_blocks(every, acts, extended, taps, gate, up, down):
+    tok, channels = acts.shape[1:]
+    vmem = pl.BlockSpec(memory_space=pltpu.VMEM)
+    shapes = (
+        jax.ShapeDtypeStruct((tok, channels), jnp.bfloat16),
+        jax.ShapeDtypeStruct((every.shape[-1], channels), jnp.float32),
+    )
+    return pl.pallas_call(
+        last_kernel,
+        out_shape=shapes
+        + tuple(jax.ShapeDtypeStruct(array.shape, array.dtype) for array in (gate, up, down)),
+        in_specs=[vmem] * 7,
+        out_specs=[pl.BlockSpec(memory_space=pltpu.HBM)] * 5,
+        scratch_shapes=[pltpu.VMEM(shape.shape, shape.dtype) for shape in shapes]
+        + [pltpu.SemaphoreType.DMA((5,))],
+        compiler_params=pltpu.CompilerParams(vmem_limit_bytes=16 * 2**20),
+        cost_estimate=pl.CostEstimate(flops=10**9, bytes_accessed=10**7, transcendentals=0),
+    )(every, acts, extended, taps, gate, up, down)
 
 
 def shards(
@@ -661,20 +727,20 @@
         experts,
         groups,
     )
-    own_cotangent = lax.dynamic_slice_in_dim(
-        cotangent, lax.axis_index("tp") * share, share, axis=1
-    )
-    result, grad_proj = tail_blocks(
+    every, acts, extended = tail_blocks(
         table.reshape(-1, table.shape[-1]),
         home_rows.reshape(-1, share),
-        own_cotangent,
+        cotangent,
         saved_normalized,
-        inverse_deviation[:, None],
+        inverse_deviation[None, :],
         channel_norm_gain[None, :],
-        taps,
         proj_weight,
+        (taps.shape[0] + 6) // 8 * 8,
         experts,
         groups,
+    )
+    result, grad_proj, grad_first, grad_third, grad_second = last_blocks(
+        every, acts, extended, taps, grad_first, grad_third, grad_second
     )
     return (
         result,

time: 103 us -> 92.5 us (0.90)
  local copies, waits for them, and re-layouts: 11.6 us -> 0.02 us
  Pallas kernels: 90.2 us -> 91.6 us
    unnamed x23 -> x10, local copies, waits for them, and re-layouts: 9.88 us -> 0.02 us
    pallas_call x0 -> x1, Pallas kernels: none -> 3.06 us  [last_blocks(): pl.pallas_call(last_kernel, out_shape=shapes + tuple((jax.ShapeDtypeStruc...]
    pallas_call x1, Pallas kernels: 67.4 us -> 66.1 us  [expert_blocks(): pl.pallas_call(functools.partial(expert_kernel, experts, groups), out_sha...]
where the time goes in v3:
time: 92.5 us; the launch traced here: 92.3 us
  Pallas kernels  91.6 us (99%)
    pallas_call x1, Pallas kernels, expert_blocks(): pl.pallas_call(functools.partial(expert_kernel, experts, groups), out_sha...  66.1 us
    pallas_call x1, Pallas kernels, tail_blocks(): pl.pallas_call(functools.partial(tail_kernel, experts, groups, lead), out...  22.4 us
    pallas_call x1, Pallas kernels, last_blocks(): pl.pallas_call(last_kernel, out_shape=shapes + tuple((jax.ShapeDtypeStruc...  3.06 us

profile of v3, /device:TPU:0, one launch (start us, length us, event | category | flops | bytes accessed | tf_op | source)
XLA Modules:
  0.0 92.3 jit_solution(15153126095401643336)
XLA Ops:
  0.6 0.0 copy-start.1
  0.6 0.0 copy-start.2
  0.7 0.0 copy-start.3
  0.7 0.0 copy-start.4
  0.7 66.1 %shard_map.155 = (bf16[8,64,512]{2,1,0:T(8,128)(2,1)S(1)}, bf16[2048,512]{1,0:T(8,128)(2,1)S(1)}, bf16[2048,512]{1,0:T(8,128)(2,1)S(1)}, bf16[512,2048]{1,0:T(8,128)(2,1)S(1)}, bf16[8,64,128]{2,1,0:T(8,128)(2,1)S(1)}) custom-call(s32[2,128]{1,0:T(2,128)} %bitcast.22, f32[2,128]{1,0:T(2,128)} %bitcast.23, bf16[128,2048]{1,0:T(8,128)(2,1)} %mixer_far.1, ...), custom_call_target="tpu_custom_call" | custom-call | flops 10000000000 | bytes 10000000 | tf_op jit(solution)/shard_map/pallas_call | solution.py:335
  66.7 0.0 copy-start
  66.8 0.0 copy-done.1
  66.8 0.0 copy-done.2
  66.8 0.0 copy-done.3
  66.8 0.0 copy-done.4
  66.8 22.4 %shard_map.156 = (bf16[8,2,64,256]{3,2,1,0:T(8,128)(2,1)S(1)}, bf16[8,128,512]{2,1,0:T(8,128)(2,1)S(1)}, f32[4,160,128]{2,1,0:T(8,128)S(1)}) custom-call(bf16[512,128]{1,0:T(8,128)(2,1)S(1)} %bitcast.15, bf16[512,512]{1,0:T(8,128)(2,1)S(1)} %bitcast.14, bf16[128,2048]{1,0:T(8,128)(2,1)} %cotangent_far.3, bf16[128,512]{1,0:T(8,128)(2,1)S(1)} %copy-done.2, ...), custom_call_target="tpu_custom_call" | custom-call | flops 1000000000 | bytes 10000000 | tf_op jit(solution)/shard_map/pallas_call | solution.py:615
  89.2 0.0 copy-done
  89.2 3.1 %shard_map.157 = (bf16[128,512]{1,0:T(8,128)(2,1)}, f32[256,512]{1,0:T(8,128)}, bf16[2048,512]{1,0:T(8,128)(2,1)}, bf16[2048,512]{1,0:T(8,128)(2,1)}, bf16[512,2048]{1,0:T(8,128)(2,1)}) custom-call(bf16[8,2,64,256]{3,2,1,0:T(8,128)(2,1)S(1)} %get-tuple-element.20.every, bf16[8,128,512]{2,1,0:T(8,128)(2,1)S(1)} %get-tuple-element.21.acts, ...), custom_call_target="tpu_custom_call" | custom-call | flops 1000000000 | bytes 10000000 | tf_op jit(solution)/shard_map/pallas_call | solution.py:689
Async XLA Ops:
  0.6 66.1 %copy-start.1 = (bf16[512,2048]{1,0:T(8,128)(2,1)S(1)}, bf16[512,2048]{1,0:T(8,128)(2,1)}, u32[]{:S(2)}) copy-start(bf16[512,2048]{1,0:T(8,128)(2,1)} %weight.1) | copy-start | bytes 6291460
  0.6 66.1 %copy-start.2 = (bf16[128,512]{1,0:T(8,128)(2,1)S(1)}, bf16[128,512]{1,0:T(8,128)(2,1)}, u32[]{:S(2)}) copy-start(bf16[128,512]{1,0:T(8,128)(2,1)} %saved.1) | copy-start | bytes 393220
  0.7 66.1 %copy-start.3 = (f32[512]{0:T(512)S(1)}, f32[512]{0:T(512)}, u32[]{:S(2)}) copy-start(f32[512]{0:T(512)} %param.18) | copy-start | bytes 6148
  0.7 66.1 %copy-start.4 = (f32[128]{0:T(128)S(1)}, f32[128]{0:T(128)}, u32[]{:S(2)}) copy-start(f32[128]{0:T(128)} %param.17) | copy-start | bytes 1540
  66.7 22.5 %copy-start = (f32[31,512]{1,0:T(8,128)S(1)}, f32[31,512]{1,0:T(8,128)}, u32[]{:S(2)}) copy-start(f32[31,512]{1,0:T(8,128)} %taps.1) | copy-start | bytes 190468

commit v4 on v3

v4 whole, which is shorter than its diff:
```python
import functools

import jax
import jax.numpy as jnp
from jax import lax
from jax.experimental import pallas as pl
from jax.experimental.pallas import tpu as pltpu
from jax.sharding import PartitionSpec as P


def line_width(experts):
    width = 1
    while 4 * width * width <= experts and experts % (2 * width) == 0:
        width = 2 * width
    return width


def sigmoid(value):
    return 1.0 / (1.0 + jnp.exp(-value))


def mate(index, step, count):
    if count & (count - 1):
        raise ValueError("count")
    value, bit = 0, 1
    while bit < count:
        value = value + bit * ((index // bit + step // bit) % 2)
        bit = 2 * bit
    return value


def remote(source, target, send_sem, recv_sem, device):
    return pltpu.make_async_remote_copy(
        src_ref=source,
        dst_ref=target,
        send_sem=send_sem,
        recv_sem=recv_sem,
        device_id=device,
        device_id_type=pl.DeviceIdType.MESH,
    )


CONTRACT_LAST = (((1,), (1,)), ((), ()))
CONTRACT_FIRST = (((0,), (0,)), ((), ()))


def expert_kernel(
    experts, groups, lead, ids_far, route_far, mixer_far, cotangent_far, gate_far, up_far, down_far,
    saved_far, gain_far, weight_far, inverse_far, grad_gate, grad_up, grad_down, acts, crossed,
    every, extended, ids, route, mixer, cotangent, saved, gain, weight, inverse, home, table,
    blocks, sums, held, sent, gate, up, down, hidden_gate, hidden_up, active,
    grad_hg, grad_hu, partial, pair_in, row_out, row_in, total, slot_weight, *sems
):
    (load_sem, far_send, far_recv, row_send, row_recv, pair_send, pair_recv,
     home_send, home_recv, sum_send, sum_recv, back_send, back_recv,
     line_send, line_recv, side_send, side_recv) = sems[:17]
    mine = lax.axis_index("sp")
    place = lax.axis_index("tp")
    chips = groups // 2
    chip, core = place // 2, place % 2
    sibling = chip * 2 + 1 - core
    tok = mixer.shape[0]
    capacity, share = held.shape[3:]
    slots = experts * capacity

    def at_chip(step):
        return ((chip + step) % chips) * 2 + core

    loads = [
        pltpu.make_async_copy(source, target, load_sem.at[at])
        for at, (source, target) in enumerate(
            (
                (ids_far, ids), (route_far, route), (mixer_far, mixer), (cotangent_far, cotangent),
                (gate_far, gate), (up_far, up), (down_far, down), (saved_far, saved),
                (gain_far, gain), (weight_far, weight), (inverse_far, inverse),
            )
        )
    ]
    for load in loads:
        load.start()
    barrier = pltpu.get_barrier_semaphore()

    def greet(step, carry):
        pl.semaphore_signal(barrier, inc=1, device_id=((mine + step) % experts, place),
                            device_id_type=pl.DeviceIdType.MESH)
        return carry

    lax.fori_loop(1, experts, greet, 0)

    def greet_group(step, carry):
        pl.semaphore_signal(barrier, inc=1, device_id=(mine, (place + step) % groups),
                            device_id_type=pl.DeviceIdType.MESH)
        return carry

    lax.fori_loop(1, groups, greet_group, 0)
    loads[0].wait()
    loads[1].wait()
    expert = lax.broadcasted_iota(jnp.int32, (experts, tok), 0)
    hot = [(ids[k : k + 1] == expert).astype(jnp.float32) for k in range(ids.shape[0])]
    before = lax.broadcasted_iota(jnp.int32, (tok, tok), 0)
    after = lax.broadcasted_iota(jnp.int32, (tok, tok), 1)
    rank = jnp.dot(
        sum(hot).astype(jnp.bfloat16),
        (before < after).astype(jnp.float32).astype(jnp.bfloat16),
        preferred_element_type=jnp.float32,
    )
    slot = expert.astype(jnp.float32) * capacity + rank
    number = lax.broadcasted_iota(jnp.int32, (slots, tok), 0).astype(jnp.float32)
    chosen = jnp.zeros((slots, tok), jnp.float32)
    weighted = jnp.zeros((slots, tok), jnp.float32)
    for k in range(ids.shape[0]):
        match = number == jnp.sum(hot[k] * slot, axis=0, keepdims=True)
        chosen = jnp.where(match, 1.0, chosen)
        weighted = jnp.where(match, route[k : k + 1], weighted)
    table[...] = chosen.astype(jnp.bfloat16).reshape(experts, capacity, tok)
    slot_weight[...] = jnp.sum(weighted, axis=1, keepdims=True).reshape(experts, capacity, 1)
    columns = pl.ds(pl.multiple_of(place * share, share), share)
    whole = table[...].reshape(slots, tok)
    scale = slot_weight[...].reshape(slots, 1)
    loads[2].wait()
    sent[:, 0] = (
        jnp.dot(whole, mixer[:, columns], preferred_element_type=jnp.float32)
        .astype(jnp.bfloat16).reshape(experts, capacity, share)
    )
    loads[3].wait()
    sent[:, 1] = (
        (scale * jnp.dot(whole, cotangent[:, columns], preferred_element_type=jnp.float32))
        .astype(jnp.bfloat16).reshape(experts, capacity, share)
    )
    pl.semaphore_wait(barrier, experts + groups - 2)

    def far(step):
        peer = mate(mine, step, experts)
        return remote(sent.at[peer], held.at[step, place],
                      far_send.at[step], far_recv.at[step], (peer, place))

    def row(step, hop):
        block = held.at[step, place]
        return remote(block, block, row_send.at[step, hop], row_recv.at[step, hop],
                      (mine, at_chip(hop)))

    def pair(step, hop):
        block = held.at[step, at_chip(chips - hop)]
        return remote(block, block, pair_send.at[step, hop], pair_recv.at[step, hop],
                      (mine, sibling))

    def each(low, high, act):
        def body(step, carry):
            act(step)
            return carry

        lax.fori_loop(low, high, body, 0)

    each(1, experts, lambda step: far(step).start())
    own = table[mine]
    own_scale = slot_weight[mine]
    for g in range(groups):
        span = slice(g * share, (g + 1) * share)
        held[0, g, 0] = jnp.dot(
            own, mixer[:, span], preferred_element_type=jnp.float32
        ).astype(jnp.bfloat16)
        held[0, g, 1] = (
            own_scale * jnp.dot(own, cotangent[:, span], preferred_element_type=jnp.float32)
        ).astype(jnp.bfloat16)

    across = experts // lead
    line, side = mine // lead, mine % lead

    def along(step, bit):
        peer = mate(line, bit, across) * lead + side
        return remote(acts.at[step], acts.at[step + bit], line_send.at[step + bit],
                      line_recv.at[step + bit], (peer, place))

    acts_order = sorted(range(1, across), key=lambda step: -(step & -step))

    def spread(step):
        bit = 1
        while bit < across:
            if step % (2 * bit) == 0:
                along(step, bit).start()
            bit = 2 * bit

    def reached(step):
        bit = 1
        while step % (2 * bit) == 0:
            bit = 2 * bit
        return along(step - bit, bit)

    def beside(step, hop):
        return remote(acts.at[step], crossed.at[hop - 1, step], side_send.at[step, hop],
                      side_recv.at[step, hop], (line * lead + mate(side, hop, lead), place))

    def cross(step):
        for hop in range(1, lead):
            beside(step, hop).start()

    def extend(step):
        reached(step).wait_recv()
        spread(step)

    def early_acts():
        spread(0)
        cross(0)

    def relay_acts():
        for step in acts_order:
            if step & (step - 1) == 0 and step > 1:
                extend(step)

    def later_acts():
        for step in acts_order:
            if step & (step - 1) or step == 1:
                extend(step)
            cross(step)

    def finish_acts():
        for step in range(1, across):
            reached(step).wait_send()
        for step in range(across):
            for hop in range(1, lead):
                beside(step, hop).wait()

    loads[7].wait()
    loads[8].wait()
    scaled = saved[...].astype(jnp.float32) * gain[...]
    acts[0] = (scaled * sigmoid(scaled)).astype(jnp.bfloat16)

    def service(step):
        far(step).wait_recv()
        for hop in range(1, chips):
            row(step, hop).start()
        pair(step, 0).start()

    def settle(step):
        for hop in range(1, chips):
            row(step, hop).wait_recv()
            pair(step, hop).start()

    def complete(step):
        for hop in range(chips):
            pair(step, hop).wait_recv()

    def chunk(kind, low, high, g):
        return held[low:high, g, kind].reshape((high - low) * capacity, share)

    def ahead(low, high):
        lines = slice(low * capacity, high * capacity)
        for matrix, result in ((gate, hidden_gate), (up, hidden_up)):
            value = None
            for g in range(groups):
                term = jnp.dot(
                    chunk(0, low, high, g), matrix[g * share : (g + 1) * share, :],
                    preferred_element_type=jnp.float32,
                )
                value = term if value is None else value + term
            result[lines, :] = value

    def back(low, high):
        lines = slice(low * capacity, high * capacity)
        value = None
        for g in range(groups):
            term = lax.dot_general(
                chunk(1, low, high, g), down[:, g * share : (g + 1) * share], CONTRACT_LAST,
                preferred_element_type=jnp.float32,
            )
            value = term if value is None else value + term
        hg = hidden_gate[lines, :]
        hu = hidden_up[lines, :]
        sigma = sigmoid(hg)
        swish = hg * sigma
        active[lines, :] = (swish * hu).astype(jnp.bfloat16)
        grad_hg[lines, :] = (value * hu * sigma * (1.0 + hg * (1.0 - sigma))).astype(jnp.bfloat16)
        grad_hu[lines, :] = (value * swish).astype(jnp.bfloat16)
        for g in range(groups):
            term = lax.dot_general(
                grad_hg[lines, :], gate[g * share : (g + 1) * share, :], CONTRACT_LAST,
                preferred_element_type=jnp.float32,
            ) + lax.dot_general(
                grad_hu[lines, :], up[g * share : (g + 1) * share, :], CONTRACT_LAST,
                preferred_element_type=jnp.float32,
            )
            partial[g, low:high] = term.astype(jnp.bfloat16).reshape(high - low, capacity, share)

    def weight_grads(g):
        span = pl.ds(pl.multiple_of(g * share, share), share)
        left = held[:, g, 0].reshape(slots, share)
        grad_gate[span, :] = lax.dot_general(
            left, grad_hg[...], CONTRACT_FIRST, preferred_element_type=jnp.float32
        ).astype(jnp.bfloat16)
        grad_up[span, :] = lax.dot_general(
            left, grad_hu[...], CONTRACT_FIRST, preferred_element_type=jnp.float32
        ).astype(jnp.bfloat16)
        grad_down[:, span] = lax.dot_general(
            active[...], held[:, g, 1].reshape(slots, share), CONTRACT_FIRST,
            preferred_element_type=jnp.float32,
        ).astype(jnp.bfloat16)

    def home_pair(step, hop):
        other = ((chip + hop) % chips) * 2 + 1 - core
        return remote(partial.at[other, step], pair_in.at[hop, step],
                      home_send.at[step, hop], home_recv.at[step, hop], (mine, sibling))

    def home_row(step, hop):
        return remote(row_out.at[hop, step], row_in.at[hop, step],
                      sum_send.at[step, hop], sum_recv.at[step, hop], (mine, at_chip(hop)))

    def home_far(step):
        owner = mate(mine, step, experts)
        return remote(total.at[step], home.at[mine],
                      back_send.at[step], back_recv.at[step], (owner, place))

    def start_pair(step):
        for hop in reversed(range(chips)):
            home_pair(step, hop).start()

    def add_pair(step, hop):
        home_pair(step, hop).wait_recv()
        return partial[at_chip(hop), step].astype(jnp.float32) + pair_in[hop, step].astype(
            jnp.float32
        )

    def send_rows(step):
        for hop in range(1, chips):
            row_out[hop, step] = add_pair(step, hop).astype(row_out.dtype)
            home_row(step, hop).start()

    def add_rows(step):
        value = add_pair(step, 0)
        for hop in range(1, chips):
            home_row(step, hop).wait_recv()
            value = value + row_in[hop, step].astype(jnp.float32)
        return value.astype(total.dtype)

    def send_home(step):
        total[step] = add_rows(step)
        home_far(step).start()

    first, second = experts // 2, 3 * experts // 4
    each(1, first, service)
    each(1, first, settle)
    for load in loads[4:7]:
        load.wait()
    each(1, first, complete)
    ahead(0, first)
    each(first, first + 1, service)
    back(0, first)
    each(0, first, start_pair)
    each(first + 1, second, service)
    each(first, first + 1, settle)
    each(second, second + 1, service)
    each(first + 1, second, settle)
    early_acts()
    each(second + 1, experts, service)
    each(0, first, send_rows)
    each(first, second, complete)
    ahead(first, second)
    back(first, second)
    each(first, second, start_pair)
    each(second, experts, settle)
    each(first, second, send_rows)
    each(second, experts, complete)
    ahead(second, experts)
    back(second, experts)
    each(second, experts, start_pair)
    home[mine] = add_rows(0)
    each(first, second, send_home)
    each(second, experts, send_rows)
    each(1, first, send_home)
    weight_grads(0)
    relay_acts()
    each(1, groups - 1, weight_grads)
    each(second, experts, send_home)
    weight_grads(groups - 1)
    later_acts()

    def return_done(step):
        home_far(step).wait_recv()

    each(1, experts, return_done)
    loads[9].wait()
    loads[10].wait()
    tail_part(
        experts, groups, mine, place, table, home, cotangent[:, columns], saved, inverse, gain,
        weight, every, extended, blocks, sums, *sems[17:],
    )

    def finish(step):
        for hop in range(chips):
            home_pair(step, hop).wait_send()
            if hop:
                home_row(step, hop).wait_send()

    def finish_far(step):
        home_far(step).wait_send()
        far(step).wait_send()
        for hop in range(chips):
            pair(step, hop).wait_send()
            if hop:
                row(step, hop).wait_send()

    finish_acts()
    each(0, experts, finish)
    each(1, experts, finish_far)


def expert_blocks(
    ids, route, mixer, cotangent, gate, up, down, saved, gain, weight, inverse, reach, experts,
    groups,
):
    tok, width = mixer.shape
    ff = gate.shape[1]
    share = width // groups
    capacity = groups * max(1, 4 * tok // (experts * groups))
    chips = groups // 2
    slots = experts * capacity
    lead = line_width(experts)
    across = experts // lead
    half = jnp.bfloat16
    dma = pltpu.SemaphoreType.DMA
    vmem = pl.BlockSpec(memory_space=pltpu.VMEM)
    held = pltpu.VMEM((experts, groups, 2, capacity, share), half)
    sent = pltpu.VMEM((experts, 2, capacity, share), half)
    kept = pltpu.VMEM((experts, capacity, share), half)
    blocks = pltpu.VMEM((chips, experts, capacity, share), half)
    channels = saved.shape[1]
    lanes = min(channels, 128)
    columns = width // experts
    outs = tuple(jax.ShapeDtypeStruct(array.shape, half) for array in (gate, up, down)) + (
        jax.ShapeDtypeStruct((across,) + saved.shape, half),
        jax.ShapeDtypeStruct((lead - 1, across) + saved.shape, half),
        jax.ShapeDtypeStruct((experts, 2, tok // 2, columns), half),
        jax.ShapeDtypeStruct((channels // lanes, tok + reach, lanes), jnp.float32),
    )
    inputs = (ids, route, mixer, cotangent, gate, up, down, saved, gain, weight, inverse)
    return pl.pallas_call(
        functools.partial(expert_kernel, experts, groups, lead),
        out_shape=outs,
        in_specs=[pl.BlockSpec(memory_space=pltpu.HBM)] * len(inputs),
        out_specs=[vmem] * len(outs),
        scratch_shapes=[
            pltpu.VMEM(array.shape, array.dtype)
            for array in (ids, route, mixer, cotangent, saved, gain, weight, inverse)
        ]
        + [
            kept,
            pltpu.VMEM((experts, capacity, tok), half),
            pltpu.VMEM((experts, 2, tok // 2, columns), half),
            pltpu.VMEM((groups, 2, 8, tok), jnp.float32),
        ]
        + [held, sent]
        + [pltpu.VMEM(array.shape, half) for array in (gate, up, down)]
        + [pltpu.VMEM((slots, ff), jnp.float32)] * 2
        + [pltpu.VMEM((slots, ff), half)] * 3
        + [pltpu.VMEM((groups, experts, capacity, share), half)]
        + [blocks] * 3
        + [kept, pltpu.VMEM((experts, capacity, 1), jnp.float32)]
        + [dma((11,))]
        + [dma((experts,))] * 2
        + [dma((experts, chips))] * 8
        + [dma((experts,))] * 2
        + [dma((across,))] * 2
        + [dma((across, lead))] * 2
        + [dma((chips,))] * 4
        + [dma((experts,))] * 4
        + [dma((groups,))] * 2
        + [dma] * 2,
        compiler_params=pltpu.CompilerParams(
            collective_id=0, has_side_effects=True, vmem_limit_bytes=42 * 2**20
        ),
        cost_estimate=pl.CostEstimate(flops=10**10, bytes_accessed=10**7, transcendentals=0),
    )(
        *(
            pltpu.with_memory_space_constraint(array, pltpu.HBM)
            for array in inputs
        )
    )


def tail_part(
    experts, groups, mine, place, table, home, cotangent, saved, inverse, gain, weight,
    every, extended, blocks, sums, *sems
):
    (row_send, row_recv, pair_send, pair_recv, far_send, far_recv, half_send, half_recv,
     sum_send, sum_recv, halo_send, halo_recv) = sems
    chips = groups // 2
    chip, core = place // 2, place % 2
    sibling = chip * 2 + 1 - core
    tok = saved.shape[0]
    channels = saved.shape[1]
    width = blocks.shape[-1]
    per = experts // groups
    half = tok // 2

    def at_chip(step):
        return ((chip + step) % chips) * 2 + core

    def share_at(owner):
        return blocks.at[pl.ds(owner * per, per)]

    def row(hop):
        return remote(share_at(place), share_at(place), row_send.at[hop], row_recv.at[hop],
                      (mine, at_chip(hop)))

    def pair(hop):
        owner = at_chip(chips - hop)
        return remote(share_at(owner), share_at(owner), pair_send.at[hop], pair_recv.at[hop],
                      (mine, sibling))

    share = lax.dot_general(
        table[...].reshape(-1, tok), home[...].reshape(-1, home.shape[-1]), CONTRACT_FIRST, preferred_element_type=jnp.float32
    )
    share = (share + cotangent.astype(jnp.float32)).astype(jnp.bfloat16)
    for part in range(per):
        piece = share[:, part * width : (part + 1) * width]
        blocks[place * per + part] = piece.reshape(2, half, width)
    for hop in range(1, chips):
        row(hop).start()
    pair(0).start()
    for hop in range(1, chips):
        row(hop).wait_recv()
        pair(hop).start()
    for hop in range(chips):
        pair(hop).wait_recv()

    def far(step):
        peer = mate(mine, step, experts)
        return remote(blocks.at[peer, core], every.at[step, core], far_send.at[step],
                      far_recv.at[step], (peer, place))

    def to_half(step):
        return remote(every.at[step, core], every.at[step, core], half_send.at[step],
                      half_recv.at[step], (mine, sibling))

    def start_far(step, carry):
        far(step).start()
        return carry

    lax.fori_loop(1, experts, start_far, 0)
    every[0] = blocks[mine]

    grad = jnp.zeros((tok, channels), jnp.float32)
    for part in range(experts):
        grad = grad + lax.dot_general(
            blocks[part].reshape(tok, width),
            weight[:, part * width : (part + 1) * width],
            (((1,), (1,)), ((), ())),
            preferred_element_type=jnp.float32,
        )
    normalized = saved[...].astype(jnp.float32)
    scaled = normalized * gain[...]
    gate = sigmoid(scaled)
    grad = grad * gate * (1.0 + scaled * (1.0 - gate)) * gain[...]
    lanes = min(channels, 128)
    first = jnp.zeros((tok, lanes), jnp.float32)
    second = jnp.zeros((tok, lanes), jnp.float32)
    for at in range(0, channels, lanes):
        first = first + grad[:, at : at + lanes]
        second = second + grad[:, at : at + lanes] * normalized[:, at : at + lanes]
    sums[place, 0] = jnp.sum(jnp.transpose(first).reshape(lanes // 8, 8, tok), axis=0)
    sums[place, 1] = jnp.sum(jnp.transpose(second).reshape(lanes // 8, 8, tok), axis=0)

    def tell(step):
        return remote(sums.at[place], sums.at[place], sum_send.at[step], sum_recv.at[step],
                      (mine, (place + step) % groups))

    def start_tell(step, carry):
        tell(step).start()
        return carry

    def wait_tell(step, carry):
        tell(step).wait()
        return carry

    lax.fori_loop(1, groups, start_tell, 0)
    lax.fori_loop(1, groups, wait_tell, 0)
    count = channels * groups
    total = jnp.sum(sums[...], axis=0)

    def column(kind):
        flat = jnp.sum(total[kind], axis=0, keepdims=True) / count
        return jnp.transpose(jnp.broadcast_to(flat, (lanes, tok)))

    mean, slope = column(0), column(1)
    deviation = jnp.transpose(jnp.broadcast_to(inverse[...], (lanes, tok)))
    for at in range(0, channels, lanes):
        extended[at // lanes, 0:tok] = deviation * (
            grad[:, at : at + lanes] - mean - normalized[:, at : at + lanes] * slope
        )
    reach = extended.shape[1] - tok

    def halo():
        return remote(extended.at[:, pl.ds(0, reach)], extended.at[:, pl.ds(tok, reach)],
                      halo_send, halo_recv, ((mine + experts - 1) % experts, place))

    @pl.when(mine > 0)
    def _():
        halo().start()

    @pl.when(mine == experts - 1)
    def _():
        extended[:, tok : tok + reach] = jnp.zeros((channels // lanes, reach, lanes), jnp.float32)

    def forward(step, carry):
        far(step).wait_recv()
        to_half(step).start()
        return carry

    lax.fori_loop(1, experts, forward, 0)

    @pl.when(mine < experts - 1)
    def _():
        halo().wait_recv()

    def arrive(step, carry):
        to_half(step).wait_recv()
        return carry

    lax.fori_loop(1, experts, arrive, 0)
    @pl.when(mine > 0)
    def _():
        halo().wait_send()

    for hop in range(chips):
        pair(hop).wait_send()
        if hop:
            row(hop).wait_send()

    def finish(step, carry):
        far(step).wait_send()
        to_half(step).wait_send()
        return carry

    lax.fori_loop(1, experts, finish, 0)


def last_kernel(
    lead, every, acts, crossed, extended, taps, gate, up, down, result_far, proj_far, gate_far, up_far, down_far,
    result, proj, sems
):
    stores = [
        pltpu.make_async_copy(source, target, sems.at[at])
        for at, (source, target) in enumerate(
            (
                (gate, gate_far), (up, up_far), (down, down_far), (result, result_far),
                (proj, proj_far),
            )
        )
    ]
    for store in stores[:3]:
        store.start()
    tok, channels = result.shape
    lanes = extended.shape[-1]
    for at in range(0, channels, lanes):
        value = jnp.zeros((tok, lanes), jnp.float32)
        for tap in range(taps.shape[0]):
            value = value + taps[tap : tap + 1, at : at + lanes] * extended[at // lanes, tap : tap + tok]
        result[:, at : at + lanes] = value.astype(result.dtype)
    stores[3].start()
    def product(hop, right):
        return lax.dot_general(
            every[:, hop].reshape(-1, every.shape[-1]),
            right.reshape(-1, channels),
            CONTRACT_FIRST,
            preferred_element_type=jnp.float32,
        )

    value = product(0, acts[...])
    for hop in range(1, lead):
        value = value + product(hop, crossed[hop - 1])
    proj[...] = value
    stores[4].start()
    for store in stores:
        store.wait()


def last_blocks(every, acts, crossed, extended, taps, gate, up, down):
    across, tok, channels = acts.shape
    lead = every.shape[0] // across
    every = every.reshape((across, lead) + every.shape[1:])
    vmem = pl.BlockSpec(memory_space=pltpu.VMEM)
    shapes = (
        jax.ShapeDtypeStruct((tok, channels), jnp.bfloat16),
        jax.ShapeDtypeStruct((every.shape[-1], channels), jnp.float32),
    )
    return pl.pallas_call(
        functools.partial(last_kernel, lead),
        out_shape=shapes
        + tuple(jax.ShapeDtypeStruct(array.shape, array.dtype) for array in (gate, up, down)),
        in_specs=[vmem] * 8,
        out_specs=[pl.BlockSpec(memory_space=pltpu.HBM)] * 5,
        scratch_shapes=[pltpu.VMEM(shape.shape, shape.dtype) for shape in shapes]
        + [pltpu.SemaphoreType.DMA((5,))],
        compiler_params=pltpu.CompilerParams(vmem_limit_bytes=16 * 2**20),
        cost_estimate=pl.CostEstimate(flops=10**9, bytes_accessed=10**7, transcendentals=0),
    )(every, acts, crossed, extended, taps, gate, up, down)


def shards(
    cotangent,
    mixer_out,
    expert_ids,
    route_weight,
    saved_normalized,
    inverse_deviation,
    channel_norm_gain,
    taps,
    proj_weight,
    gate_weight,
    up_weight,
    down_weight,
):
    experts = lax.axis_size("sp")
    groups = lax.axis_size("tp")
    grad_first, grad_third, grad_second, acts, crossed, every, extended = expert_blocks(
        jnp.transpose(expert_ids),
        jnp.transpose(route_weight),
        mixer_out,
        cotangent,
        gate_weight[0],
        up_weight[0],
        down_weight[0],
        saved_normalized,
        channel_norm_gain[None, :],
        proj_weight,
        inverse_deviation[None, :],
        (taps.shape[0] + 6) // 8 * 8,
        experts,
        groups,
    )
    result, grad_proj, grad_first, grad_third, grad_second = last_blocks(
        every, acts, crossed, extended, taps, grad_first, grad_third, grad_second
    )
    return (
        result,
        grad_proj,
        grad_first[None],
        grad_third[None],
        grad_second[None],
    )


def solution(mesh):
    return jax.shard_map(
        shards,
        mesh=mesh,
        in_specs=(
            P("sp", None),
            P("sp", None),
            P("sp", None),
            P("sp", None),
            P("sp", "tp"),
            P("sp"),
            P("tp"),
            P(None, "tp"),
            P("tp", None),
            P("sp", None, "tp"),
            P("sp", None, "tp"),
            P("sp", "tp", None),
        ),
        out_specs=(
            P("sp", "tp"),
            P("sp", "tp"),
            P("sp", None, "tp"),
            P("sp", None, "tp"),
            P("sp", "tp", None),
        ),
        check_vma=False,
    )
```

time: 92.5 us -> 80.4 us (0.87)
  Pallas kernels: 91.6 us -> 79.6 us
    pallas_call x3 -> x2, Pallas kernels: 91.6 us -> 79.6 us  [the longest x1 76.5 us: expert_blocks(): pl.pallas_call(functools.partial(expert_kernel, experts, groups, lead), o...]
where the time goes in v4:
time: 80.4 us; the launch traced here: 80.2 us
  Pallas kernels  79.6 us (99%)
    pallas_call x1, Pallas kernels, expert_blocks(): pl.pallas_call(functools.partial(expert_kernel, experts, groups, lead), o...  76.5 us
    pallas_call x1, Pallas kernels, last_blocks(): pl.pallas_call(functools.partial(last_kernel, lead), out_shape=shapes + t...  3.06 us

profile of v4, /device:TPU:0, one launch (start us, length us, event | category | flops | bytes accessed | tf_op | source)
XLA Modules:
  0.0 80.2 jit_solution(6870318175711700443)
XLA Ops:
  0.6 0.0 copy-start
  0.6 76.5 %shard_map.155 = (bf16[2048,512]{1,0:T(8,128)(2,1)S(1)}, bf16[2048,512]{1,0:T(8,128)(2,1)S(1)}, bf16[512,2048]{1,0:T(8,128)(2,1)S(1)}, bf16[4,128,512]{2,1,0:T(8...) custom-call(s32[2,128]{1,0:T(2,128)} %bitcast.19, ...), custom_call_target="tpu_custom_call" | custom-call | flops 10000000000 | bytes 10000000 | tf_op jit(solution)/shard_map/pallas_call | solution.py:435
  77.1 0.0 copy-done
  77.2 3.1 %shard_map.156 = (bf16[128,512]{1,0:T(8,128)(2,1)}, f32[256,512]{1,0:T(8,128)}, bf16[2048,512]{1,0:T(8,128)(2,1)}, bf16[2048,512]{1,0:T(8,128)(2,1)}, bf16[512,2048]{1,0:T(8,128)(2,1)}) custom-call(bf16[4,2,2,64,256]{4,3,2,1,0:T(8,128)(2,1)S(1)} %bitcast.11, bf16[4,128,512]{2,1,0:T(8,128)(2,1)S(1)} %get-tuple-element.18.acts, ...), custom_call_target="tpu_custom_call" | custom-call | flops 1000000000 | bytes 10000000 | tf_op jit(solution)/shard_map/pallas_call | solution.py:685
Async XLA Ops:
  0.6 76.5 %copy-start = (f32[31,512]{1,0:T(8,128)S(1)}, f32[31,512]{1,0:T(8,128)}, u32[]{:S(2)}) copy-start(f32[31,512]{1,0:T(8,128)} %taps.1) | copy-start | bytes 190468

commit v5 on v4

--- a/solution.py
+++ b/solution.py
@@ -337,40 +337,40 @@
 
     first, second = experts // 2, 3 * experts // 4
     each(1, first, service)
-    each(1, first, settle)
+    each(1, 2, settle)
+    each(first, second, service)
+    each(2, second, settle)
     for load in loads[4:7]:
         load.wait()
-    each(1, first, complete)
-    ahead(0, first)
-    each(first, first + 1, service)
-    back(0, first)
-    each(0, first, start_pair)
-    each(first + 1, second, service)
-    each(first, first + 1, settle)
-    each(second, second + 1, service)
-    each(first + 1, second, settle)
-    early_acts()
-    each(second + 1, experts, service)
-    each(0, first, send_rows)
     each(first, second, complete)
     ahead(first, second)
     back(first, second)
     each(first, second, start_pair)
+    each(second, second + 1, service)
+    each(1, first, complete)
+    ahead(0, first)
+    each(second + 1, experts, service)
+    each(first, second, send_rows)
+    early_acts()
+    back(0, first)
+    each(0, first, start_pair)
     each(second, experts, settle)
-    each(first, second, send_rows)
+    each(0, first // 2, send_rows)
     each(second, experts, complete)
     ahead(second, experts)
     back(second, experts)
     each(second, experts, start_pair)
+    each(first, second, send_home)
+    weight_grads(0)
+    each(second, experts, send_rows)
+    each(first // 2, first, send_rows)
     home[mine] = add_rows(0)
-    each(first, second, send_home)
-    each(second, experts, send_rows)
-    each(1, first, send_home)
-    weight_grads(0)
+    each(1, first // 2, send_home)
     relay_acts()
     each(1, groups - 1, weight_grads)
     each(second, experts, send_home)
     weight_grads(groups - 1)
+    each(first // 2, first, send_home)
     later_acts()
 
     def return_done(step):
@@ -513,39 +513,55 @@
     for part in range(per):
         piece = share[:, part * width : (part + 1) * width]
         blocks[place * per + part] = piece.reshape(2, half, width)
-    for hop in range(1, chips):
-        row(hop).start()
-    pair(0).start()
-    for hop in range(1, chips):
-        row(hop).wait_recv()
-        pair(hop).start()
-    for hop in range(chips):
-        pair(hop).wait_recv()
-
     def far(step):
         peer = mate(mine, step, experts)
         return remote(blocks.at[peer, core], every.at[step, core], far_send.at[step],
                       far_recv.at[step], (peer, place))
 
     def to_half(step):
-        return remote(every.at[step, core], every.at[step, core], half_send.at[step],
-                      half_recv.at[step], (mine, sibling))
-
-    def start_far(step, carry):
-        far(step).start()
-        return carry
-
-    lax.fori_loop(1, experts, start_far, 0)
+        return remote(every.at[step, core], every.at[step, core],
+                      half_send.at[step], half_recv.at[step], (mine, sibling))
+
+    def send_share(owner):
+        for part in range(per):
+            peer = owner * per + part
+
+            @pl.when(peer != mine)
+            def _(peer=peer):
+                far(mate(mine, peer, experts)).start()
+
+    def product(owner):
+        side = weight[:, pl.ds(pl.multiple_of(owner * per * width, per * width), per * width)]
+        value = None
+        for part in range(per):
+            term = lax.dot_general(
+                blocks[owner * per + part].reshape(tok, width),
+                side[:, part * width : (part + 1) * width],
+                CONTRACT_LAST,
+                preferred_element_type=jnp.float32,
+            )
+            value = term if value is None else value + term
+        return value
+
+    for hop in range(1, chips):
+        row(hop).start()
+    pair(0).start()
+    send_share(place)
+    grad = product(place)
+    pair(0).wait_recv()
+    send_share(sibling)
+    grad = grad + product(sibling)
+    for hop in range(1, chips):
+        row(hop).wait_recv()
+        pair(hop).start()
+        send_share(at_chip(chips - hop))
+        grad = grad + product(at_chip(chips - hop))
+    for hop in range(1, chips):
+        pair(hop).wait_recv()
+        other = ((chip + chips - hop) % chips) * 2 + 1 - core
+        send_share(other)
+        grad = grad + product(other)
     every[0] = blocks[mine]
-
-    grad = jnp.zeros((tok, channels), jnp.float32)
-    for part in range(experts):
-        grad = grad + lax.dot_general(
-            blocks[part].reshape(tok, width),
-            weight[:, part * width : (part + 1) * width],
-            (((1,), (1,)), ((), ())),
-            preferred_element_type=jnp.float32,
-        )
     normalized = saved[...].astype(jnp.float32)
     scaled = normalized * gain[...]
     gate = sigmoid(scaled)

time: 80.4 us -> 75.2 us (0.935)
  Pallas kernels: 79.6 us -> 74.4 us
    pallas_call x1, Pallas kernels: 76.5 us -> 71.3 us  [expert_blocks(): pl.pallas_call(functools.partial(expert_kernel, experts, groups, lead), o...]
where the time goes in v5:
time: 75.2 us; the launch traced here: 75.1 us
  Pallas kernels  74.4 us (99%)
    pallas_call x1, Pallas kernels, expert_blocks(): pl.pallas_call(functools.partial(expert_kernel, experts, groups, lead), o...  71.3 us
    pallas_call x1, Pallas kernels, last_blocks(): pl.pallas_call(functools.partial(last_kernel, lead), out_shape=shapes + t...  3.07 us

profile of v5, /device:TPU:0, one launch (start us, length us, event | category | flops | bytes accessed | tf_op | source)
XLA Modules:
  0.0 75.1 jit_solution(1059318017568461074)
XLA Ops:
  0.6 0.0 copy-start
  0.6 71.3 %shard_map.155 = (bf16[2048,512]{1,0:T(8,128)(2,1)S(1)}, bf16[2048,512]{1,0:T(8,128)(2,1)S(1)}, bf16[512,2048]{1,0:T(8,128)(2,1)S(1)}, bf16[4,128,512]{2,1,0:T(8...) custom-call(s32[2,128]{1,0:T(2,128)} %bitcast.19, ...), custom_call_target="tpu_custom_call" | custom-call | flops 10000000000 | bytes 10000000 | tf_op jit(solution)/shard_map/pallas_call | solution.py:435
  72.0 0.0 copy-done
  72.0 3.1 %shard_map.156 = (bf16[128,512]{1,0:T(8,128)(2,1)}, f32[256,512]{1,0:T(8,128)}, bf16[2048,512]{1,0:T(8,128)(2,1)}, bf16[2048,512]{1,0:T(8,128)(2,1)}, bf16[512,2048]{1,0:T(8,128)(2,1)}) custom-call(bf16[4,2,2,64,256]{4,3,2,1,0:T(8,128)(2,1)S(1)} %bitcast.11, bf16[4,128,512]{2,1,0:T(8,128)(2,1)S(1)} %get-tuple-element.18.acts, ...), custom_call_target="tpu_custom_call" | custom-call | flops 1000000000 | bytes 10000000 | tf_op jit(solution)/shard_map/pallas_call | solution.py:701
Async XLA Ops:
  0.6 71.4 %copy-start = (f32[31,512]{1,0:T(8,128)S(1)}, f32[31,512]{1,0:T(8,128)}, u32[]{:S(2)}) copy-start(f32[31,512]{1,0:T(8,128)} %taps.1) | copy-start | bytes 190468

commit v6 on v5

--- a/solution.py
+++ b/solution.py
@@ -48,12 +48,13 @@
     experts, groups, lead, ids_far, route_far, mixer_far, cotangent_far, gate_far, up_far, down_far,
     saved_far, gain_far, weight_far, inverse_far, grad_gate, grad_up, grad_down, acts, crossed,
     every, extended, ids, route, mixer, cotangent, saved, gain, weight, inverse, home, table,
-    blocks, sums, held, sent, gate, up, down, hidden_gate, hidden_up, active,
+    blocks, sums, tokens, ids_in, route_in, relayed, more, held, sent, gate, up, down, hidden_gate, hidden_up, active,
     grad_hg, grad_hu, partial, pair_in, row_out, row_in, total, slot_weight, *sems
 ):
     (load_sem, far_send, far_recv, row_send, row_recv, pair_send, pair_recv,
      home_send, home_recv, sum_send, sum_recv, back_send, back_recv,
-     line_send, line_recv, side_send, side_recv) = sems[:17]
+     line_send, line_recv, side_send, side_recv, token_send, token_recv, relay_send,
+     relay_recv) = sems[:21]
     mine = lax.axis_index("sp")
     place = lax.axis_index("tp")
     chips = groups // 2
@@ -93,45 +94,62 @@
         return carry
 
     lax.fori_loop(1, groups, greet_group, 0)
-    loads[0].wait()
-    loads[1].wait()
-    expert = lax.broadcasted_iota(jnp.int32, (experts, tok), 0)
-    hot = [(ids[k : k + 1] == expert).astype(jnp.float32) for k in range(ids.shape[0])]
-    before = lax.broadcasted_iota(jnp.int32, (tok, tok), 0)
-    after = lax.broadcasted_iota(jnp.int32, (tok, tok), 1)
-    rank = jnp.dot(
-        sum(hot).astype(jnp.bfloat16),
-        (before < after).astype(jnp.float32).astype(jnp.bfloat16),
-        preferred_element_type=jnp.float32,
-    )
-    slot = expert.astype(jnp.float32) * capacity + rank
-    number = lax.broadcasted_iota(jnp.int32, (slots, tok), 0).astype(jnp.float32)
-    chosen = jnp.zeros((slots, tok), jnp.float32)
-    weighted = jnp.zeros((slots, tok), jnp.float32)
-    for k in range(ids.shape[0]):
-        match = number == jnp.sum(hot[k] * slot, axis=0, keepdims=True)
-        chosen = jnp.where(match, 1.0, chosen)
-        weighted = jnp.where(match, route[k : k + 1], weighted)
-    table[...] = chosen.astype(jnp.bfloat16).reshape(experts, capacity, tok)
-    slot_weight[...] = jnp.sum(weighted, axis=1, keepdims=True).reshape(experts, capacity, 1)
+    first = experts // 2
+    base = mine // first * first
     columns = pl.ds(pl.multiple_of(place * share, share), share)
-    whole = table[...].reshape(slots, tok)
-    scale = slot_weight[...].reshape(slots, 1)
-    loads[2].wait()
-    sent[:, 0] = (
-        jnp.dot(whole, mixer[:, columns], preferred_element_type=jnp.float32)
-        .astype(jnp.bfloat16).reshape(experts, capacity, share)
-    )
-    loads[3].wait()
+    for load in loads[:4]:
+        load.wait()
+    pl.semaphore_wait(barrier, experts + groups - 2)
+    opposite = mate(mine, first, experts)
+    crossing = [
+        remote(source, target, token_send.at[at], token_recv.at[at], (opposite, place))
+        for at, (source, target) in enumerate(
+            (
+                (ids, ids_in), (route, route_in), (mixer.at[:, columns], tokens.at[0]),
+                (cotangent.at[:, columns], tokens.at[1]),
+            )
+        )
+    ]
+    crossing[0].start()
+    crossing[1].start()
+
+    def slot_table(chosen_ids, weights, low, count):
+        expert = lax.broadcasted_iota(jnp.int32, (experts, tok), 0)
+        hot = [(chosen_ids[k : k + 1] == expert).astype(jnp.float32) for k in range(ids.shape[0])]
+        before = lax.broadcasted_iota(jnp.int32, (tok, tok), 0)
+        after = lax.broadcasted_iota(jnp.int32, (tok, tok), 1)
+        rank = jnp.dot(
+            sum(hot).astype(jnp.bfloat16),
+            (before < after).astype(jnp.float32).astype(jnp.bfloat16),
+            preferred_element_type=jnp.float32,
+        )
+        slot = expert.astype(jnp.float32) * capacity + rank
+        number = (lax.broadcasted_iota(jnp.int32, (count, tok), 0) + low).astype(jnp.float32)
+        chosen = jnp.zeros((count, tok), jnp.float32)
+        weighted = jnp.zeros((count, tok), jnp.float32)
+        for k in range(ids.shape[0]):
+            match = number == jnp.sum(hot[k] * slot, axis=0, keepdims=True)
+            chosen = jnp.where(match, 1.0, chosen)
+            weighted = jnp.where(match, weights[k : k + 1], weighted)
+        return chosen.astype(jnp.bfloat16), jnp.sum(weighted, axis=1, keepdims=True)
+
+    def pick(picks, values):
+        return jnp.dot(picks, values, preferred_element_type=jnp.float32)
+
+    every_slot, scale = slot_table(ids[...], route[...], 0, slots)
+    table[...] = every_slot.reshape(experts, capacity, tok)
+    slot_weight[...] = scale.reshape(experts, capacity, 1)
+    near = table[pl.ds(base, first)].reshape(first * capacity, tok)
+    near_scale = slot_weight[pl.ds(base, first)].reshape(first * capacity, 1)
+    sent[:, 0] = pick(near, mixer[:, columns]).astype(jnp.bfloat16).reshape(first, capacity, share)
     sent[:, 1] = (
-        (scale * jnp.dot(whole, cotangent[:, columns], preferred_element_type=jnp.float32))
-        .astype(jnp.bfloat16).reshape(experts, capacity, share)
-    )
-    pl.semaphore_wait(barrier, experts + groups - 2)
+        (near_scale * pick(near, cotangent[:, columns]))
+        .astype(jnp.bfloat16).reshape(first, capacity, share)
+    )
 
     def far(step):
         peer = mate(mine, step, experts)
-        return remote(sent.at[peer], held.at[step, place],
+        return remote(sent.at[peer - base], held.at[step, place],
                       far_send.at[step], far_recv.at[step], (peer, place))
 
     def row(step, hop):
@@ -151,7 +169,30 @@
 
         lax.fori_loop(low, high, body, 0)
 
-    each(1, experts, lambda step: far(step).start())
+    def extra(step, hop):
+        return remote(more.at[hop - 1, step - 1], held.at[step, at_chip(chips - hop)],
+                      row_send.at[step, hop], row_recv.at[step, hop],
+                      (mate(mine, step, experts), place))
+
+    each(1, first, lambda step: far(step).start())
+    for hop in range(1, chips):
+        other = pl.ds(pl.multiple_of(at_chip(chips - hop) * share, share), share)
+        for step in range(1, lead):
+            peer = mate(mine, step, experts)
+            picks = table[peer]
+            more[hop - 1, step - 1, 0] = pick(picks, mixer[:, other]).astype(jnp.bfloat16)
+            more[hop - 1, step - 1, 1] = (
+                slot_weight[peer] * pick(picks, cotangent[:, other])
+            ).astype(jnp.bfloat16)
+            extra(step, hop).start()
+    crossing[2].start()
+    crossing[3].start()
+
+    def relay(kind, step):
+        peer = mate(mine, step, experts)
+        return remote(relayed.at[peer - base, kind], held.at[step + first, place, kind],
+                      relay_send.at[kind, step], relay_recv.at[kind, step], (peer, place))
+
     own = table[mine]
     own_scale = slot_weight[mine]
     for g in range(groups):
@@ -225,8 +266,20 @@
     scaled = saved[...].astype(jnp.float32) * gain[...]
     acts[0] = (scaled * sigmoid(scaled)).astype(jnp.bfloat16)
 
+    def greeted(step):
+        far(step).wait_recv()
+        pair(step, 0).start()
+
     def service(step):
         far(step).wait_recv()
+        hand_on(step)
+
+    def serve(step):
+        relay(0, step - first).wait_recv()
+        relay(1, step - first).wait_recv()
+        hand_on(step)
+
+    def hand_on(step):
         for hop in range(1, chips):
             row(step, hop).start()
         pair(step, 0).start()
@@ -242,6 +295,19 @@
 
     def chunk(kind, low, high, g):
         return held[low:high, g, kind].reshape((high - low) * capacity, share)
+
+    crossing[0].wait_recv()
+    crossing[1].wait_recv()
+    far_table, far_scale = slot_table(ids_in[...], route_in[...], base * capacity, first * capacity)
+
+    def relay_kind(kind):
+        crossing[kind + 2].wait_recv()
+        value = pick(far_table, tokens[kind])
+        if kind:
+            value = far_scale * value
+        relayed[:, kind] = value.astype(jnp.bfloat16).reshape(first, capacity, share)
+        each(1, first, lambda step: relay(kind, step).start())
+        held[first, place, kind] = relayed[mine - base, kind]
 
     def ahead(low, high):
         lines = slice(low * capacity, high * capacity)
@@ -335,26 +401,29 @@
         total[step] = add_rows(step)
         home_far(step).start()
 
-    first, second = experts // 2, 3 * experts // 4
-    each(1, first, service)
-    each(1, 2, settle)
-    each(first, second, service)
-    each(2, second, settle)
+    second = 3 * experts // 4
+    each(1, lead, greeted)
+    each(lead, first, service)
+    relay_kind(0)
+    relay_kind(1)
+    hand_on(first)
+    each(1, first, settle)
+    each(first + 1, second, serve)
     for load in loads[4:7]:
         load.wait()
+    each(1, first, complete)
+    ahead(0, first)
+    each(second, experts, serve)
+    back(0, first)
+    each(0, first, start_pair)
+    early_acts()
+    each(first, second, settle)
     each(first, second, complete)
     ahead(first, second)
     back(first, second)
     each(first, second, start_pair)
-    each(second, second + 1, service)
-    each(1, first, complete)
-    ahead(0, first)
-    each(second + 1, experts, service)
+    each(second, experts, settle)
     each(first, second, send_rows)
-    early_acts()
-    back(0, first)
-    each(0, first, start_pair)
-    each(second, experts, settle)
     each(0, first // 2, send_rows)
     each(second, experts, complete)
     ahead(second, experts)
@@ -381,7 +450,7 @@
     loads[10].wait()
     tail_part(
         experts, groups, mine, place, table, home, cotangent[:, columns], saved, inverse, gain,
-        weight, every, extended, blocks, sums, *sems[17:],
+        weight, every, extended, blocks, sums, *sems[21:],
     )
 
     def finish(step):
@@ -392,7 +461,6 @@
 
     def finish_far(step):
         home_far(step).wait_send()
-        far(step).wait_send()
         for hop in range(chips):
             pair(step, hop).wait_send()
             if hop:
@@ -401,6 +469,15 @@
     finish_acts()
     each(0, experts, finish)
     each(1, experts, finish_far)
+
+    def finish_near(step):
+        far(step).wait_send()
+        relay(0, step).wait_send()
+        relay(1, step).wait_send()
+
+    each(1, first, finish_near)
+    for copy in crossing:
+        copy.wait_send()
 
 
 def expert_blocks(
@@ -419,7 +496,7 @@
     dma = pltpu.SemaphoreType.DMA
     vmem = pl.BlockSpec(memory_space=pltpu.VMEM)
     held = pltpu.VMEM((experts, groups, 2, capacity, share), half)
-    sent = pltpu.VMEM((experts, 2, capacity, share), half)
+    sent = pltpu.VMEM((experts // 2, 2, capacity, share), half)
     kept = pltpu.VMEM((experts, capacity, share), half)
     blocks = pltpu.VMEM((chips, experts, capacity, share), half)
     channels = saved.shape[1]
@@ -446,6 +523,11 @@
             pltpu.VMEM((experts, capacity, tok), half),
             pltpu.VMEM((experts, 2, tok // 2, columns), half),
             pltpu.VMEM((groups, 2, 8, tok), jnp.float32),
+            pltpu.VMEM((2, tok, share), half),
+            pltpu.VMEM(ids.shape, ids.dtype),
+            pltpu.VMEM(route.shape, route.dtype),
+            sent,
+            pltpu.VMEM((chips - 1, lead - 1, 2, capacity, share), half),
         ]
         + [held, sent]
         + [pltpu.VMEM(array.shape, half) for array in (gate, up, down)]
@@ -460,6 +542,8 @@
         + [dma((experts,))] * 2
         + [dma((across,))] * 2
         + [dma((across, lead))] * 2
+        + [dma((4,))] * 2
+        + [dma((2, experts // 2))] * 2
         + [dma((chips,))] * 4
         + [dma((experts,))] * 4
         + [dma((groups,))] * 2

time: 75.2 us -> 71.4 us (0.949)
  Pallas kernels: 74.4 us -> 70.6 us
    pallas_call x1, Pallas kernels: 71.3 us -> 67.5 us  [expert_blocks(): pl.pallas_call(functools.partial(expert_kernel, experts, groups, lead), o...]
where the time goes in v6:
time: 71.4 us; the launch traced here: 71.3 us
  Pallas kernels  70.6 us (99%)
    pallas_call x1, Pallas kernels, expert_blocks(): pl.pallas_call(functools.partial(expert_kernel, experts, groups, lead), o...  67.5 us
    pallas_call x1, Pallas kernels, last_blocks(): pl.pallas_call(functools.partial(last_kernel, lead), out_shape=shapes + t...  3.07 us

profile of v6, /device:TPU:0, one launch (start us, length us, event | category | flops | bytes accessed | tf_op | source)
XLA Modules:
  0.0 71.3 jit_solution(12218428128869206973)
XLA Ops:
  0.6 0.0 copy-start
  0.6 67.5 %shard_map.155 = (bf16[2048,512]{1,0:T(8,128)(2,1)S(1)}, bf16[2048,512]{1,0:T(8,128)(2,1)S(1)}, bf16[512,2048]{1,0:T(8,128)(2,1)S(1)}, bf16[4,128,512]{2,1,0:T(8...) custom-call(s32[2,128]{1,0:T(2,128)} %bitcast.19, ...), custom_call_target="tpu_custom_call" | custom-call | flops 10000000000 | bytes 10000000 | tf_op jit(solution)/shard_map/pallas_call | solution.py:512
  68.2 0.0 copy-done
  68.2 3.1 %shard_map.156 = (bf16[128,512]{1,0:T(8,128)(2,1)}, f32[256,512]{1,0:T(8,128)}, bf16[2048,512]{1,0:T(8,128)(2,1)}, bf16[2048,512]{1,0:T(8,128)(2,1)}, bf16[512,2048]{1,0:T(8,128)(2,1)}) custom-call(bf16[4,2,2,64,256]{4,3,2,1,0:T(8,128)(2,1)S(1)} %bitcast.11, bf16[4,128,512]{2,1,0:T(8,128)(2,1)S(1)} %get-tuple-element.18.acts, ...), custom_call_target="tpu_custom_call" | custom-call | flops 1000000000 | bytes 10000000 | tf_op jit(solution)/shard_map/pallas_call | solution.py:785
Async XLA Ops:
  0.6 67.5 %copy-start = (f32[31,512]{1,0:T(8,128)S(1)}, f32[31,512]{1,0:T(8,128)}, u32[]{:S(2)}) copy-start(f32[31,512]{1,0:T(8,128)} %taps.1) | copy-start | bytes 190468

commit v7 on v6

--- a/solution.py
+++ b/solution.py
@@ -46,9 +46,9 @@
 
 def expert_kernel(
     experts, groups, lead, ids_far, route_far, mixer_far, cotangent_far, gate_far, up_far, down_far,
-    saved_far, gain_far, weight_far, inverse_far, grad_gate, grad_up, grad_down, acts, crossed,
-    every, extended, ids, route, mixer, cotangent, saved, gain, weight, inverse, home, table,
-    blocks, sums, tokens, ids_in, route_in, relayed, more, held, sent, gate, up, down, hidden_gate, hidden_up, active,
+    saved_far, gain_far, weight_far, inverse_far, taps_far, grad_gate, grad_up, grad_down, acts,
+    crossed, every, extended, head, ids, route, mixer, cotangent, saved, gain, weight, inverse, taps, home, table,
+    blocks, sums, tokens, ids_in, route_in, relayed, more, held, sent, gate_t, up_t, down_t, gate, up, down, hidden_gate, hidden_up, active,
     grad_hg, grad_hu, partial, pair_in, row_out, row_in, total, slot_weight, *sems
 ):
     (load_sem, far_send, far_recv, row_send, row_recv, pair_send, pair_recv,
@@ -74,6 +74,7 @@
                 (ids_far, ids), (route_far, route), (mixer_far, mixer), (cotangent_far, cotangent),
                 (gate_far, gate), (up_far, up), (down_far, down), (saved_far, saved),
                 (gain_far, gain), (weight_far, weight), (inverse_far, inverse),
+                (taps_far, taps),
             )
         )
     ]
@@ -309,6 +310,15 @@
         each(1, first, lambda step: relay(kind, step).start())
         held[first, place, kind] = relayed[mine - base, kind]
 
+    def turn_weights():
+        for load in loads[4:7]:
+            load.wait()
+        for g in range(groups):
+            span = slice(g * share, (g + 1) * share)
+            gate_t[:, span] = jnp.transpose(gate[span, :])
+            up_t[:, span] = jnp.transpose(up[span, :])
+            down_t[span, :] = jnp.transpose(down[:, span])
+
     def ahead(low, high):
         lines = slice(low * capacity, high * capacity)
         for matrix, result in ((gate, hidden_gate), (up, hidden_up)):
@@ -325,8 +335,8 @@
         lines = slice(low * capacity, high * capacity)
         value = None
         for g in range(groups):
-            term = lax.dot_general(
-                chunk(1, low, high, g), down[:, g * share : (g + 1) * share], CONTRACT_LAST,
+            term = jnp.dot(
+                chunk(1, low, high, g), down_t[g * share : (g + 1) * share, :],
                 preferred_element_type=jnp.float32,
             )
             value = term if value is None else value + term
@@ -338,11 +348,11 @@
         grad_hg[lines, :] = (value * hu * sigma * (1.0 + hg * (1.0 - sigma))).astype(jnp.bfloat16)
         grad_hu[lines, :] = (value * swish).astype(jnp.bfloat16)
         for g in range(groups):
-            term = lax.dot_general(
-                grad_hg[lines, :], gate[g * share : (g + 1) * share, :], CONTRACT_LAST,
+            term = jnp.dot(
+                grad_hg[lines, :], gate_t[:, g * share : (g + 1) * share],
                 preferred_element_type=jnp.float32,
-            ) + lax.dot_general(
-                grad_hu[lines, :], up[g * share : (g + 1) * share, :], CONTRACT_LAST,
+            ) + jnp.dot(
+                grad_hu[lines, :], up_t[:, g * share : (g + 1) * share],
                 preferred_element_type=jnp.float32,
             )
             partial[g, low:high] = term.astype(jnp.bfloat16).reshape(high - low, capacity, share)
@@ -403,14 +413,13 @@
 
     second = 3 * experts // 4
     each(1, lead, greeted)
+    turn_weights()
     each(lead, first, service)
     relay_kind(0)
     relay_kind(1)
     hand_on(first)
     each(1, first, settle)
     each(first + 1, second, serve)
-    for load in loads[4:7]:
-        load.wait()
     each(1, first, complete)
     ahead(0, first)
     each(second, experts, serve)
@@ -422,8 +431,9 @@
     ahead(first, second)
     back(first, second)
     each(first, second, start_pair)
-    each(second, experts, settle)
+    each(second, second + 1, settle)
     each(first, second, send_rows)
+    each(second + 1, experts, settle)
     each(0, first // 2, send_rows)
     each(second, experts, complete)
     ahead(second, experts)
@@ -433,11 +443,11 @@
     weight_grads(0)
     each(second, experts, send_rows)
     each(first // 2, first, send_rows)
-    home[mine] = add_rows(0)
-    each(1, first // 2, send_home)
     relay_acts()
     each(1, groups - 1, weight_grads)
     each(second, experts, send_home)
+    home[mine] = add_rows(0)
+    each(1, first // 2, send_home)
     weight_grads(groups - 1)
     each(first // 2, first, send_home)
     later_acts()
@@ -448,9 +458,10 @@
     each(1, experts, return_done)
     loads[9].wait()
     loads[10].wait()
+    loads[11].wait()
     tail_part(
         experts, groups, mine, place, table, home, cotangent[:, columns], saved, inverse, gain,
-        weight, every, extended, blocks, sums, *sems[21:],
+        weight, taps, every, extended, head, blocks, sums, *sems[21:],
     )
 
     def finish(step):
@@ -481,7 +492,7 @@
 
 
 def expert_blocks(
-    ids, route, mixer, cotangent, gate, up, down, saved, gain, weight, inverse, reach, experts,
+    ids, route, mixer, cotangent, gate, up, down, saved, gain, weight, inverse, taps, experts,
     groups,
 ):
     tok, width = mixer.shape
@@ -502,13 +513,15 @@
     channels = saved.shape[1]
     lanes = min(channels, 128)
     columns = width // experts
+    reach = (taps.shape[0] + 6) // 8 * 8
     outs = tuple(jax.ShapeDtypeStruct(array.shape, half) for array in (gate, up, down)) + (
         jax.ShapeDtypeStruct((across,) + saved.shape, half),
         jax.ShapeDtypeStruct((lead - 1, across) + saved.shape, half),
         jax.ShapeDtypeStruct((experts, 2, tok // 2, columns), half),
         jax.ShapeDtypeStruct((channels // lanes, tok + reach, lanes), jnp.float32),
-    )
-    inputs = (ids, route, mixer, cotangent, gate, up, down, saved, gain, weight, inverse)
+        jax.ShapeDtypeStruct((tok - reach, channels), half),
+    )
+    inputs = (ids, route, mixer, cotangent, gate, up, down, saved, gain, weight, inverse, taps)
     return pl.pallas_call(
         functools.partial(expert_kernel, experts, groups, lead),
         out_shape=outs,
@@ -516,7 +529,7 @@
         out_specs=[vmem] * len(outs),
         scratch_shapes=[
             pltpu.VMEM(array.shape, array.dtype)
-            for array in (ids, route, mixer, cotangent, saved, gain, weight, inverse)
+            for array in (ids, route, mixer, cotangent, saved, gain, weight, inverse, taps)
         ]
         + [
             kept,
@@ -530,13 +543,14 @@
             pltpu.VMEM((chips - 1, lead - 1, 2, capacity, share), half),
         ]
         + [held, sent]
+        + [pltpu.VMEM(array.shape[::-1], half) for array in (gate, up, down)]
         + [pltpu.VMEM(array.shape, half) for array in (gate, up, down)]
         + [pltpu.VMEM((slots, ff), jnp.float32)] * 2
         + [pltpu.VMEM((slots, ff), half)] * 3
         + [pltpu.VMEM((groups, experts, capacity, share), half)]
         + [blocks] * 3
         + [kept, pltpu.VMEM((experts, capacity, 1), jnp.float32)]
-        + [dma((11,))]
+        + [dma((12,))]
         + [dma((experts,))] * 2
         + [dma((experts, chips))] * 8
         + [dma((experts,))] * 2
@@ -560,9 +574,18 @@
     )
 
 
+def convolve(taps, extended, at, lanes, low, rows):
+    value = jnp.zeros((rows, lanes), jnp.float32)
+    for tap in range(taps.shape[0]):
+        value = value + taps[tap : tap + 1, at : at + lanes] * (
+            extended[at // lanes, low + tap : low + tap + rows]
+        )
+    return value
+
+
 def tail_part(
     experts, groups, mine, place, table, home, cotangent, saved, inverse, gain, weight,
-    every, extended, blocks, sums, *sems
+    taps, every, extended, head, blocks, sums, *sems
 ):
     (row_send, row_recv, pair_send, pair_recv, far_send, far_recv, half_send, half_recv,
      sum_send, sum_recv, halo_send, halo_recv) = sems
@@ -706,6 +729,10 @@
         return carry
 
     lax.fori_loop(1, experts, forward, 0)
+    for at in range(0, channels, lanes):
+        head[:, at : at + lanes] = convolve(
+            taps, extended, at, lanes, 0, head.shape[0]
+        ).astype(head.dtype)
 
     @pl.when(mine < experts - 1)
     def _():
@@ -734,26 +761,25 @@
 
 
 def last_kernel(
-    lead, every, acts, crossed, extended, taps, gate, up, down, result_far, proj_far, gate_far, up_far, down_far,
+    lead, every, acts, crossed, extended, head, taps, gate, up, down, result_far, proj_far, gate_far, up_far, down_far,
     result, proj, sems
 ):
     stores = [
         pltpu.make_async_copy(source, target, sems.at[at])
         for at, (source, target) in enumerate(
             (
-                (gate, gate_far), (up, up_far), (down, down_far), (result, result_far),
-                (proj, proj_far),
+                (gate, gate_far), (up, up_far), (down, down_far), (result, result_far.at[pl.ds(head.shape[0], result.shape[0])]),
+                (proj, proj_far), (head, result_far.at[pl.ds(0, head.shape[0])]),
             )
         )
     ]
     for store in stores[:3]:
         store.start()
-    tok, channels = result.shape
+    stores[5].start()
+    rows, channels = result.shape
     lanes = extended.shape[-1]
     for at in range(0, channels, lanes):
-        value = jnp.zeros((tok, lanes), jnp.float32)
-        for tap in range(taps.shape[0]):
-            value = value + taps[tap : tap + 1, at : at + lanes] * extended[at // lanes, tap : tap + tok]
+        value = convolve(taps, extended, at, lanes, head.shape[0], rows)
         result[:, at : at + lanes] = value.astype(result.dtype)
     stores[3].start()
     def product(hop, right):
@@ -773,7 +799,7 @@
         store.wait()
 
 
-def last_blocks(every, acts, crossed, extended, taps, gate, up, down):
+def last_blocks(every, acts, crossed, extended, head, taps, gate, up, down):
     across, tok, channels = acts.shape
     lead = every.shape[0] // across
     every = every.reshape((across, lead) + every.shape[1:])
@@ -786,13 +812,16 @@
         functools.partial(last_kernel, lead),
         out_shape=shapes
         + tuple(jax.ShapeDtypeStruct(array.shape, array.dtype) for array in (gate, up, down)),
-        in_specs=[vmem] * 8,
+        in_specs=[vmem] * 9,
         out_specs=[pl.BlockSpec(memory_space=pltpu.HBM)] * 5,
-        scratch_shapes=[pltpu.VMEM(shape.shape, shape.dtype) for shape in shapes]
-        + [pltpu.SemaphoreType.DMA((5,))],
+        scratch_shapes=[
+            pltpu.VMEM((tok - head.shape[0], channels), jnp.bfloat16),
+            pltpu.VMEM(shapes[1].shape, jnp.float32),
+        ]
+        + [pltpu.SemaphoreType.DMA((6,))],
         compiler_params=pltpu.CompilerParams(vmem_limit_bytes=16 * 2**20),
         cost_estimate=pl.CostEstimate(flops=10**9, bytes_accessed=10**7, transcendentals=0),
-    )(every, acts, crossed, extended, taps, gate, up, down)
+    )(every, acts, crossed, extended, head, taps, gate, up, down)
 
 
 def shards(
@@ -811,7 +840,7 @@
 ):
     experts = lax.axis_size("sp")
     groups = lax.axis_size("tp")
-    grad_first, grad_third, grad_second, acts, crossed, every, extended = expert_blocks(
+    grad_first, grad_third, grad_second, acts, crossed, every, extended, head = expert_blocks(
         jnp.transpose(expert_ids),
         jnp.transpose(route_weight),
         mixer_out,
@@ -823,12 +852,12 @@
         channel_norm_gain[None, :],
         proj_weight,
         inverse_deviation[None, :],
-        (taps.shape[0] + 6) // 8 * 8,
+        taps,
         experts,
         groups,
     )
     result, grad_proj, grad_first, grad_third, grad_second = last_blocks(
-        every, acts, crossed, extended, taps, grad_first, grad_third, grad_second
+        every, acts, crossed, extended, head, taps, grad_first, grad_third, grad_second
     )
     return (
         result,

time: 71.4 us -> 70.4 us (0.986)
  Pallas kernels: 70.6 us -> 69.6 us
    pallas_call x1, Pallas kernels: 67.5 us -> 66.7 us  [expert_blocks(): pl.pallas_call(functools.partial(expert_kernel, experts, groups, lead), o...]
where the time goes in v7:
time: 70.4 us; the launch traced here: 70.3 us
  Pallas kernels  69.6 us (99%)
    pallas_call x1, Pallas kernels, expert_blocks(): pl.pallas_call(functools.partial(expert_kernel, experts, groups, lead), o...  66.7 us
    pallas_call x1, Pallas kernels, last_blocks(): pl.pallas_call(functools.partial(last_kernel, lead), out_shape=shapes + t...  2.92 us

profile of v7, /device:TPU:0, one launch (start us, length us, event | category | flops | bytes accessed | tf_op | source)
XLA Modules:
  0.0 70.3 jit_solution(1992357298474455170)
XLA Ops:
  0.6 0.0 copy-start
  0.6 66.7 %shard_map.155 = (bf16[2048,512]{1,0:T(8,128)(2,1)S(1)}, bf16[2048,512]{1,0:T(8,128)(2,1)S(1)}, bf16[512,2048]{1,0:T(8,128)(2,1)S(1)}, bf16[4,128,512]{2,1,0:T(8...) custom-call(s32[2,128]{1,0:T(2,128)} %bitcast.19, ...), custom_call_target="tpu_custom_call" | custom-call | flops 10000000000 | bytes 10000000 | tf_op jit(solution)/shard_map/pallas_call | solution.py:525
  67.4 0.0 copy-done
  67.4 2.9 %shard_map.156 = (bf16[128,512]{1,0:T(8,128)(2,1)}, f32[256,512]{1,0:T(8,128)}, bf16[2048,512]{1,0:T(8,128)(2,1)}, bf16[2048,512]{1,0:T(8,128)(2,1)}, bf16[512,2048]{1,0:T(8,128)(2,1)}) custom-call(bf16[4,2,2,64,256]{4,3,2,1,0:T(8,128)(2,1)S(1)} %bitcast.11, bf16[4,128,512]{2,1,0:T(8,128)(2,1)S(1)} %get-tuple-element.19.acts, ...), custom_call_target="tpu_custom_call" | custom-call | flops 1000000000 | bytes 10000000 | tf_op jit(solution)/shard_map/pallas_call | solution.py:811
Async XLA Ops:
  0.6 66.7 %copy-start = (f32[31,512]{1,0:T(8,128)S(1)}, f32[31,512]{1,0:T(8,128)}, u32[]{:S(2)}) copy-start(f32[31,512]{1,0:T(8,128)} %taps.1) | copy-start | bytes 190468

commit v8 on v7

--- a/solution.py
+++ b/solution.py
@@ -421,8 +421,9 @@
     each(1, first, settle)
     each(first + 1, second, serve)
     each(1, first, complete)
+    each(second, second + 1, serve)
     ahead(0, first)
-    each(second, experts, serve)
+    each(second + 1, experts, serve)
     back(0, first)
     each(0, first, start_pair)
     early_acts()

time: 70.4 us -> 70.3 us (level)
  no operation moved by 1% of the time
where the time goes in v8:
time: 70.3 us; the launch traced here: 70.1 us
  Pallas kernels  69.5 us (99%)
    pallas_call x1, Pallas kernels, expert_blocks(): pl.pallas_call(functools.partial(expert_kernel, experts, groups, lead), o...  66.5 us
    pallas_call x1, Pallas kernels, last_blocks(): pl.pallas_call(functools.partial(last_kernel, lead), out_shape=shapes + t...  2.92 us

profile of v8, /device:TPU:0, one launch (start us, length us, event | category | flops | bytes accessed | tf_op | source)
XLA Modules:
  0.0 70.1 jit_solution(15334084091071659562)
XLA Ops:
  0.6 0.0 copy-start
  0.6 66.5 %shard_map.155 = (bf16[2048,512]{1,0:T(8,128)(2,1)S(1)}, bf16[2048,512]{1,0:T(8,128)(2,1)S(1)}, bf16[512,2048]{1,0:T(8,128)(2,1)S(1)}, bf16[4,128,512]{2,1,0:T(8...) custom-call(s32[2,128]{1,0:T(2,128)} %bitcast.19, ...), custom_call_target="tpu_custom_call" | custom-call | flops 10000000000 | bytes 10000000 | tf_op jit(solution)/shard_map/pallas_call | solution.py:526
  67.2 0.0 copy-done
  67.2 2.9 %shard_map.156 = (bf16[128,512]{1,0:T(8,128)(2,1)}, f32[256,512]{1,0:T(8,128)}, bf16[2048,512]{1,0:T(8,128)(2,1)}, bf16[2048,512]{1,0:T(8,128)(2,1)}, bf16[512,2048]{1,0:T(8,128)(2,1)}) custom-call(bf16[4,2,2,64,256]{4,3,2,1,0:T(8,128)(2,1)S(1)} %bitcast.11, bf16[4,128,512]{2,1,0:T(8,128)(2,1)S(1)} %get-tuple-element.19.acts, ...), custom_call_target="tpu_custom_call" | custom-call | flops 1000000000 | bytes 10000000 | tf_op jit(solution)/shard_map/pallas_call | solution.py:812
Async XLA Ops:
  0.6 66.6 %copy-start = (f32[31,512]{1,0:T(8,128)S(1)}, f32[31,512]{1,0:T(8,128)}, u32[]{:S(2)}) copy-start(f32[31,512]{1,0:T(8,128)} %taps.1) | copy-start | bytes 190468
